TPU v7x, 128 devices: a whole 4x4x4 slice. The times are simulated.
128 devices in a mesh: kv: 16 (over z, x), tp: 8 (over y, core).
Axes of the slice: x: 4, y: 4, z: 4, core: 2. Of those that a mesh axis runs over, the one named last changes fastest.
Arguments:
- tokens: bfloat16 [128, 4096], P('tp', 'kv'), may hold values from -16 to 16
- cache_keys: bfloat16 [128, 16384, 2, 128], P('tp', 'kv'), may hold values from -512 to 512
- cache_values: bfloat16 [128, 16384, 2, 128], P('tp', 'kv'), may hold values from -6 to 6
- attn_gain: float32 [4096], P('kv'), may hold values from 0.1 to 1.9
- w_query: bfloat16 [4096, 2048], P('kv'), may hold values from -0.15625 to 0.15625
- w_key: bfloat16 [4096, 256], P('kv'), may hold values from -0.09375 to 0.09375
- w_value: bfloat16 [4096, 256], P('kv'), may hold values from -0.09375 to 0.09375
- lambdas: float32 [16], replicated, may hold values from 0.3 to 0.8
- head_gain: float32 [128], replicated, may hold values from 0.1 to 1.9
- w_out: bfloat16 [2048, 4096], P(None, 'kv'), may hold values from -0.125 to 0.125
- mlp_gain: float32 [4096], P('kv'), may hold values from 0.1 to 1.9
- w_up: bfloat16 [4096, 16384], P('kv', 'tp'), may hold values from -0.09375 to 0.09375
- w_down: bfloat16 [16384, 4096], P('tp', 'kv'), may hold values from -0.046875 to 0.046875
Outputs:
- mixed: bfloat16 [128, 4096], P('tp', 'kv')
- new_keys: bfloat16 [128, 2, 128], P('tp')
- new_values: bfloat16 [128, 2, 128], P('tp')
All inputs are finite; a program needn't handle non-finite values.
Results may differ from a plain program's by a relative error of at most 0.014.
Values may be sent and summed in bfloat16 or wider, within the bound.
No kernel may reach another device: no remote copies, remote signals or barrier semaphores. Data moves between devices by JAX's collectives and lax.ppermute only.
A program may use at most 128 MiB of HBM per device.

v0:
```python
import functools

import jax
import jax.numpy as jnp
from jax import lax
from jax.sharding import Mesh
from jax.sharding import PartitionSpec as P

KV = ("kv_0", "kv_1")


norm_eps = 1e-06


def from_everyone(shard, axis):
    peers = lax.axis_size(axis)
    return lax.all_to_all(
        jnp.broadcast_to(shard[None], (peers, *shard.shape)), axis, 0, 0, tiled=True
    )


def of_everyone(shard, axis):
    everything = from_everyone(shard, axis)
    return jnp.sum(everything, axis=0)


def packed_total(arrays, axis):
    ravelled, at, gathered = (jnp.concatenate([a.reshape(-1) for a in arrays]), 0, [])
    total = of_everyone(ravelled, axis)
    for a in arrays:
        gathered.append(total[at : at + a.size].reshape(a.shape))
        at += a.size
    return tuple(gathered)


def by_axis(shard, axes):
    return functools.reduce(lax.pmax, axes, shard)


def cut_along(shard, dim, peers):
    before, after = (shard.shape[:dim], shard.shape[dim + 1 :])
    return jnp.moveaxis(shard.reshape(*before, peers, -1, *after), dim, 0)


def sum_at_owner(shard, axis, dim):
    tiles = cut_along(shard, dim, lax.axis_size(axis))
    arrived = lax.all_to_all(tiles, axis, split_axis=0, concat_axis=0, tiled=True)
    return arrived.sum(axis=0)


def in_one_piece(arrays, axis, dim, along):
    columns = [a.reshape(*a.shape[:along], -1) for a in arrays]
    both = jnp.concatenate(columns, axis=along)
    whole, at, gathered = (sum_at_owner(both, axis, dim), 0, [])
    for a, column in zip(arrays, columns):
        slab = whole[..., at : at + column.shape[along]]
        gathered.append(slab.reshape(*slab.shape[:along], *a.shape[along:]))
        at += column.shape[along]
    return tuple(gathered)


def laid_out(tiles, dim):
    shape = list(tiles.shape[1:])
    shape[dim] *= tiles.shape[0]
    return jnp.moveaxis(tiles, 0, dim).reshape(shape)


def gathered_copies(shard, axis, dim):
    tiles = from_everyone(shard, axis)
    return laid_out(tiles, dim)


def by_axis_2(shard, axes):
    return functools.reduce(lax.psum, axes, shard)


def sent_and_summed(shard, axis, dim):
    tiles = cut_along(shard, dim, lax.axis_size(axis))
    arrived = lax.all_to_all(tiles, axis, split_axis=0, concat_axis=0, tiled=True)
    return arrived.astype(jnp.float32).sum(axis=0)


def head_norm(acc, total, lam_heads, head_gain, ctx_total):
    head_out = (
        acc[..., 0, :] / total[..., 0, None] - lam_heads * acc[..., 1, :] / total[..., 1, None]
    )
    mean_sq = jnp.mean(head_out * head_out, axis=-1, keepdims=True)
    return (head_out * lax.rsqrt(mean_sq + 1.0 / ctx_total) * head_gain).astype(jnp.bfloat16)


def shards(
    tokens,
    cache_keys,
    cache_values,
    attn_gain,
    w_query,
    w_key,
    w_value,
    lambdas,
    head_gain,
    w_out,
    mlp_gain,
    w_up,
    w_down,
):
    tok_rows, tok_width = tokens.shape
    full_width = tok_width * lax.axis_size(KV)
    tok_f = tokens.astype(jnp.float32)
    scaled = (tok_f * attn_gain[None, :]).astype(jnp.bfloat16)
    squares = jnp.sum(tok_f * tok_f, axis=1)
    q_part = jnp.dot(scaled, w_query, preferred_element_type=jnp.float32)
    k_part = jnp.dot(scaled, w_key, preferred_element_type=jnp.float32)
    v_part = jnp.dot(scaled, w_value, preferred_element_type=jnp.float32)
    q_sum, k_sum, v_sum, sq_sum = packed_total((q_part, k_part, v_part, squares), KV)
    inv_one = lax.rsqrt(sq_sum / full_width + norm_eps)[:, None]
    query = (q_sum * inv_one).astype(jnp.bfloat16)
    new_keys = (k_sum * inv_one).astype(jnp.bfloat16)
    new_values = (v_sum * inv_one).astype(jnp.bfloat16)
    kv_heads = cache_keys.shape[2]
    comp_dim = cache_keys.shape[3] // 2
    value_dim = cache_values.shape[3]
    ctx_local = cache_keys.shape[1]
    heads = lambdas.shape[0]
    head_group = heads // kv_heads
    ctx_total = ctx_local * lax.axis_size(KV)
    query_five = query.reshape(tok_rows, kv_heads, head_group, 2, comp_dim)
    keys_five = cache_keys.reshape(tok_rows, ctx_local, kv_heads, 2, comp_dim)
    scores = jnp.einsum(
        "bkgcd,bpkcd->bkgcp", query_five, keys_five, preferred_element_type=jnp.float32
    ) * comp_dim ** (-0.5)
    block_top = jnp.max(scores, axis=-1)
    exp_scores = jnp.exp(scores - block_top[..., None])
    block_total = jnp.sum(exp_scores, axis=-1)
    weights = exp_scores.astype(jnp.bfloat16)
    block_acc = jnp.einsum(
        "bkgcp,bpke->bkgce", weights, cache_values, preferred_element_type=jnp.float32
    )
    peak = by_axis(block_top, KV)
    factor = jnp.exp(block_top - peak)
    total_part = (block_total * factor).reshape(tok_rows, heads, 2)
    acc_part = (block_acc * factor[..., None]).reshape(tok_rows, heads, 2, value_dim)
    total_own, acc_own = in_one_piece((total_part, acc_part), KV, 1, 3)
    local_heads = heads // lax.axis_size(KV)
    lam_own = lax.dynamic_slice_in_dim(lambdas, lax.axis_index(KV) * local_heads, local_heads, 0)
    normed_own = head_norm(acc_own, total_own, lam_own[None, :, None], head_gain, ctx_total)
    normed_own = normed_own.reshape(tok_rows, local_heads * value_dim)
    attn_out = jnp.dot(
        gathered_copies(normed_own, KV, 1), w_out, preferred_element_type=jnp.float32
    )
    residual = (tok_f + attn_out).astype(jnp.bfloat16)
    everyone = gathered_copies(residual, "tp", 0)
    every_f = everyone.astype(jnp.float32)
    gained = (every_f * mlp_gain[None, :]).astype(jnp.bfloat16)
    row_sq = jnp.sum(every_f * every_f, axis=1)
    up_part = jnp.dot(gained, w_up, preferred_element_type=jnp.float32)
    up_share = sum_at_owner(up_part, KV, 1)
    sq_all = by_axis_2(row_sq, KV)
    pre_act = up_share * lax.rsqrt(sq_all / full_width + norm_eps)[:, None]
    act_share = jnp.square(jax.nn.relu(pre_act)).astype(jnp.bfloat16)
    down_part = jnp.dot(
        gathered_copies(act_share, KV, 1), w_down, preferred_element_type=jnp.float32
    )
    ffn_out = sent_and_summed(down_part.astype(jnp.bfloat16), "tp", 0)
    mixed = (residual.astype(jnp.float32) + ffn_out).astype(jnp.bfloat16)
    return (
        mixed,
        new_keys.reshape(tok_rows, kv_heads, 2 * comp_dim),
        new_values.reshape(tok_rows, kv_heads, value_dim),
    )


def solution(mesh):
    split = Mesh(mesh.devices.reshape(4, 4, mesh.shape["tp"]), ("kv_0", "kv_1", "tp"))
    placed = (
        P("tp", KV),
        P("tp", KV, None, None),
        P("tp", KV, None, None),
        P(KV),
        P(KV, None),
        P(KV, None),
        P(KV, None),
        P(),
        P(),
        P(None, KV),
        P(KV),
        P(KV, "tp"),
        P("tp", KV),
    )
    return jax.shard_map(
        shards,
        mesh=split,
        in_specs=placed,
        out_specs=(P("tp", KV), P("tp", None, None), P("tp", None, None)),
        check_vma=False,
    )
```

profile of v0, /device:TPU:1, one launch (start us, length us, event | category | flops | bytes accessed | tf_op | source)
XLA Modules:
  0.0 199.1 jit_solution(12297447962373909848)
XLA Ops:
  2.9 1.1 convolution_bitcast_fusion.3
  5.1 2.9 %broadcast_in_dim.8 = f32[16,1,40976]{2,1,0:T(1,128)} broadcast(f32[40976]{0:T(1024)S(1)} %pad_maximum_fusion), dimensions={2} | broadcast | bytes 2786368 | tf_op jit(solution)/shard_map/broadcast_in_dim | solution.py:18
  8.0 8.5 %all-to-all-start = ((f32[16,1,40976]{2,1,0:T(1,128)}), f32[16,1,40976]{2,1,0:T(1,128)}, u32[]{:S(2)}, u32[]{:S(2)}) async-start(f32[16,1,40976]{2,1,0:T(1,128)} %broadcast_in_dim.8), calls=%async_computation | async-start | bytes 5259264 | tf_op jit(solution)/shard_map/all_to_all | solution.py:17
  16.5 21.2 %copy.73 = bf16[16,1024,2,128]{1,3,2,0:T(8,128)(2,1)} copy(bf16[16,1024,2,128]{3,2,1,0:T(2,128)(2,1)} %param.14) | data formatting | bytes 16777216 | tf_op args[1]
  37.6 18.1 %all-to-all-done = f32[16,1,40976]{2,1,0:T(1,128)} async-done(((f32[16,1,40976]{2,1,0:T(1,128)}), f32[16,1,40976]{2,1,0:T(1,128)}, u32[]{:S(2)}, u32[]{:S(2)}) %all-to-all-start) | async-done | bytes 2622496 | tf_op jit(solution)/shard_map/all_to_all | solution.py:17
  55.7 3.4 %reduce_sum.77 = f32[40976]{0:T(1024)S(1)} reduce(f32[16,1,40976]{2,1,0:T(1,128)} %all-to-all-done, f32[]{:T(128)} %constant.12.clone.1), dimensions={0,1}, to_apply=%region_1.0 | reduce | flops 614640 | bytes 2786372 | tf_op jit(solution)/shard_map/reduce_sum | solution.py:24
  59.8 4.7 %bitcast_reduce_fusion = (f32[16,2,8,2]{2,3,1,0:T(2,128)S(1)}, f32[16,2,2,8,1024]{4,3,2,1,0:T(8,128)S(1)}) fusion(bf16[16,1024,2,2,64]{1,4,3,2,0:T(8,128)(2,1)} %bitcast.73, f32[16,2,8,2,64]{4,3,2,1,0:T(2,128)S(1)} %reshape.295, f32[16]{0:T(128)S(1)} %fusion.26), kind=kOutput, calls=%fused_computation.3 | convolution fusion | flops 68222464 | bytes 10618944 | tf_op jit(solution)/shard_map/bkgcd,bpkcd->bkgcp/dot_general | solution.py:128
  64.5 12.3 %pmax.14 = f32[16,2,8,2]{2,3,1,0:T(2,128)S(1)} all-reduce(f32[16,2,8,2]{2,3,1,0:T(2,128)S(1)} %get-tuple-element.15), channel_id=1, replica_groups=mesh['kv_0'=4,'kv_1'=4,'tp'=8] {'kv_0'}, use_global_device_ids=true, to_apply=%region_4.0 | all-reduce | flops 512 | bytes 4096 | tf_op jit(solution)/shard_map/pmax | solution.py:37
  77.4 11.2 %pmax.15 = f32[16,2,8,2]{2,3,1,0:T(2,128)S(1)} all-reduce(f32[16,2,8,2]{2,3,1,0:T(2,128)S(1)} %pmax.14), channel_id=1, replica_groups=mesh['kv_0'=4,'kv_1'=4,'tp'=8] {'kv_1'}, use_global_device_ids=true, to_apply=%region_5.0 | all-reduce | flops 512 | bytes 4096 | tf_op jit(solution)/shard_map/pmax | solution.py:37
  88.6 4.8 %fusion.5 = f32[16,2,8,2,128]{4,2,3,1,0:T(8,128)S(1)} fusion(bf16[16,1024,2,128,1]{3,2,1,0,4:T(2,128)(2,1)} %bitcast.92, f32[16,2,2,8,1024]{4,3,2,1,0:T(8,128)S(1)} %get-tuple-element.16, f32[16,2,8,2]{2,3,1,0:T(2,128)S(1)} %get-tuple-element.15, f32[16,2,8,2]{2,3,1,0:T(2,128)S(1)} %get-tuple-element.4), kind=kOutput, calls=%fused_computation.8 | convolution fusion | flops 135856128 | bytes 10752000 | tf_op jit(solution)/shard_map/bkgcp,bpke->bkgce/dot_general | solution.py:135
  94.1 1.2 copy.78
  95.3 3.6 %all-to-all-start.1 = ((f32[16,16,1,2,129]{4,3,1,2,0:T(2,128)}), f32[16,16,1,2,129]{4,3,1,2,0:T(2,128)S(1)}, u32[]{:S(2)}, u32[]{:S(2)}) async-start(f32[16,16,1,2,129]{4,3,1,2,0:T(2,128)} %copy.78), calls=%async_computation.1 | async-start | bytes 1048576 | tf_op jit(solution)/shard_map/all_to_all | solution.py:47
  99.5 8.3 %all-to-all-done.1 = f32[16,16,1,2,129]{4,3,1,2,0:T(2,128)S(1)} async-done(((f32[16,16,1,2,129]{4,3,1,2,0:T(2,128)}), f32[16,16,1,2,129]{4,3,1,2,0:T(2,128)S(1)}, u32[]{:S(2)}, u32[]{:S(2)}) %all-to-all-start.1) | async-done | bytes 264224 | tf_op jit(solution)/shard_map/all_to_all | solution.py:47
  109.3 9.2 %all_to_all.36 = bf16[16,16,128]{2,1,0:T(8,128)(2,1)S(1)} all-to-all(bf16[16,16,128]{2,1,0:T(8,128)(2,1)S(1)} %broadcast_in_dim.9), channel_id=1, replica_groups=mesh['kv_0'=4,'kv_1'=4,'tp'=8] {'kv_0','kv_1'}, dimensions={0} | all-to-all | bytes 131072 | tf_op jit(solution)/shard_map/all_to_all | solution.py:17
  119.4 16.3 %all-to-all-start.3 = ((bf16[8,16,256]{2,1,0:T(8,128)(2,1)}), bf16[8,16,256]{2,1,0:T(8,128)(2,1)S(1)}, u32[]{:S(2)}, u32[]{:S(2)}) async-start(bf16[8,16,256]{2,1,0:T(8,128)(2,1)} %broadcast_in_dim.10), calls=%async_computation.3 | async-start | bytes 131072 | tf_op jit(solution)/shard_map/all_to_all | solution.py:17
  136.2 4.3 %all-to-all-done.3 = bf16[8,16,256]{2,1,0:T(8,128)(2,1)S(1)} async-done(((bf16[8,16,256]{2,1,0:T(8,128)(2,1)}), bf16[8,16,256]{2,1,0:T(8,128)(2,1)S(1)}, u32[]{:S(2)}, u32[]{:S(2)}) %all-to-all-start.3) | async-done | bytes 65568 | tf_op jit(solution)/shard_map/all_to_all | solution.py:17
  140.6 1.5 convolution_bitcast_fusion
  142.1 3.8 %all-to-all-start.4 = ((f32[16,128,128]{2,1,0:T(8,128)}), f32[16,128,128]{2,1,0:T(8,128)S(1)}, u32[]{:S(2)}, u32[]{:S(2)}) async-start(f32[16,128,128]{2,1,0:T(8,128)} %convolution_bitcast_fusion), calls=%async_computation.4 | async-start | bytes 2097152 | tf_op jit(solution)/shard_map/all_to_all | solution.py:47
  146.0 12.5 %psum.14 = f32[128]{0:T(128)S(1)} all-reduce(f32[128]{0:T(128)S(1)} %reduce_sum.84), channel_id=1, replica_groups=mesh['kv_0'=4,'kv_1'=4,'tp'=8] {'kv_0'}, use_global_device_ids=true, to_apply=%region_10.0 | all-reduce | flops 128 | bytes 1024 | tf_op jit(solution)/shard_map/psum | solution.py:74
  158.5 11.9 %psum.15 = f32[128]{0:T(128)S(1)} all-reduce(f32[128]{0:T(128)S(1)} %psum.14), channel_id=1, replica_groups=mesh['kv_0'=4,'kv_1'=4,'tp'=8] {'kv_1'}, use_global_device_ids=true, to_apply=%region_11.0 | all-reduce | flops 128 | bytes 1024 | tf_op jit(solution)/shard_map/psum | solution.py:74
  171.6 3.6 %all-to-all-start.5 = ((bf16[16,128,128]{1,2,0:T(8,128)(2,1)}), bf16[16,128,128]{1,2,0:T(8,128)(2,1)S(1)}, u32[]{:S(2)}, u32[]{:S(2)}) async-start(bf16[16,128,128]{1,2,0:T(8,128)(2,1)} %broadcast_in_dim.11), calls=%async_computation.5 | async-start | bytes 1048576 | tf_op jit(solution)/shard_map/all_to_all | solution.py:17
  175.9 8.3 %all-to-all-done.5 = bf16[16,128,128]{1,2,0:T(8,128)(2,1)S(1)} async-done(((bf16[16,128,128]{1,2,0:T(8,128)(2,1)}), bf16[16,128,128]{1,2,0:T(8,128)(2,1)S(1)}, u32[]{:S(2)}, u32[]{:S(2)}) %all-to-all-start.5) | async-done | bytes 524320 | tf_op jit(solution)/shard_map/all_to_all | solution.py:17
  185.2 8.4 %all-to-all-start.6 = ((bf16[8,16,256]{2,1,0:T(8,128)(2,1)}), bf16[8,16,256]{2,1,0:T(8,128)(2,1)S(1)}, u32[]{:S(2)}, u32[]{:S(2)}) async-start(bf16[8,16,256]{2,1,0:T(8,128)(2,1)} %bitcast.24), calls=%async_computation.6 | async-start | bytes 131072 | tf_op jit(solution)/shard_map/all_to_all | solution.py:79
  194.3 4.2 %all-to-all-done.6 = bf16[8,16,256]{2,1,0:T(8,128)(2,1)S(1)} async-done(((bf16[8,16,256]{2,1,0:T(8,128)(2,1)}), bf16[8,16,256]{2,1,0:T(8,128)(2,1)S(1)}, u32[]{:S(2)}, u32[]{:S(2)}) %all-to-all-start.6) | async-done | bytes 65568 | tf_op jit(solution)/shard_map/all_to_all | solution.py:79
  (60 shorter events, 13.1 us)
Async XLA Ops:
  0.6 1.2 copy-start
  8.0 47.7 %all-to-all-start = ((f32[16,1,40976]{2,1,0:T(1,128)}), f32[16,1,40976]{2,1,0:T(1,128)}, u32[]{:S(2)}, u32[]{:S(2)}) async-start(f32[16,1,40976]{2,1,0:T(1,128)} %broadcast_in_dim.8), calls=%async_computation | async-start | bytes 5259264 | tf_op jit(solution)/shard_map/all_to_all | solution.py:17
  59.1 0.7 copy-start.4
  93.4 5.5 %copy-start.8 = (f32[16]{0:T(128)S(1)}, f32[16]{0:T(128)}, u32[]{:S(2)}) copy-start(f32[16]{0:T(128)} %param.20) | copy-start | bytes 196
  93.5 15.8 %copy-start.7 = (f32[128]{0:T(128)S(1)}, f32[128]{0:T(128)}, u32[]{:S(2)}) copy-start(f32[128]{0:T(128)} %param.21) | copy-start | bytes 1540
  93.9 24.6 %copy-start.1 = (bf16[2048,256]{1,0:T(8,128)(2,1)S(1)}, bf16[2048,256]{1,0:T(8,128)(2,1)}, u32[]{:S(2)}) copy-start(bf16[2048,256]{1,0:T(8,128)(2,1)} %param.22) | copy-start | bytes 3145732
  93.9 24.6 %copy-start.5 = (bf16[16,256]{1,0:T(8,128)(2,1)S(1)}, bf16[16,256]{1,0:T(8,128)(2,1)}, u32[]{:S(2)}) copy-start(bf16[16,256]{1,0:T(8,128)(2,1)} %param.13) | copy-start | bytes 24580
  95.3 12.5 %all-to-all-start.1 = ((f32[16,16,1,2,129]{4,3,1,2,0:T(2,128)}), f32[16,16,1,2,129]{4,3,1,2,0:T(2,128)S(1)}, u32[]{:S(2)}, u32[]{:S(2)}) async-start(f32[16,16,1,2,129]{4,3,1,2,0:T(2,128)} %copy.78), calls=%async_computation.1 | async-start | bytes 1048576 | tf_op jit(solution)/shard_map/all_to_all | solution.py:47
  99.5 41.0 %copy-start.6 = (f32[256]{0:T(256)S(1)}, f32[256]{0:T(256)}, u32[]{:S(2)}) copy-start(f32[256]{0:T(256)} %param.23) | copy-start | bytes 3076
  108.1 27.6 %copy-start.2 = (bf16[256,2048]{1,0:T(8,128)(2,1)S(1)}, bf16[256,2048]{1,0:T(8,128)(2,1)}, u32[]{:S(2)}) copy-start(bf16[256,2048]{1,0:T(8,128)(2,1)} %param.24) | copy-start | bytes 3145732
  119.4 21.1 %all-to-all-start.3 = ((bf16[8,16,256]{2,1,0:T(8,128)(2,1)}), bf16[8,16,256]{2,1,0:T(8,128)(2,1)S(1)}, u32[]{:S(2)}, u32[]{:S(2)}) async-start(bf16[8,16,256]{2,1,0:T(8,128)(2,1)} %broadcast_in_dim.10), calls=%async_computation.3 | async-start | bytes 131072 | tf_op jit(solution)/shard_map/all_to_all | solution.py:17
  142.1 42.1 %copy-start.3 = (bf16[2048,256]{1,0:T(8,128)(2,1)S(1)}, bf16[2048,256]{1,0:T(8,128)(2,1)}, u32[]{:S(2)}) copy-start(bf16[2048,256]{1,0:T(8,128)(2,1)} %param.25) | copy-start | bytes 3145732
  142.1 28.3 %all-to-all-start.4 = ((f32[16,128,128]{2,1,0:T(8,128)}), f32[16,128,128]{2,1,0:T(8,128)S(1)}, u32[]{:S(2)}, u32[]{:S(2)}) async-start(f32[16,128,128]{2,1,0:T(8,128)} %convolution_bitcast_fusion), calls=%async_computation.4 | async-start | bytes 2097152 | tf_op jit(solution)/shard_map/all_to_all | solution.py:47
  171.6 12.6 %all-to-all-start.5 = ((bf16[16,128,128]{1,2,0:T(8,128)(2,1)}), bf16[16,128,128]{1,2,0:T(8,128)(2,1)S(1)}, u32[]{:S(2)}, u32[]{:S(2)}) async-start(bf16[16,128,128]{1,2,0:T(8,128)(2,1)} %broadcast_in_dim.11), calls=%async_computation.5 | async-start | bytes 1048576 | tf_op jit(solution)/shard_map/all_to_all | solution.py:17
  185.2 13.3 %all-to-all-start.6 = ((bf16[8,16,256]{2,1,0:T(8,128)(2,1)}), bf16[8,16,256]{2,1,0:T(8,128)(2,1)S(1)}, u32[]{:S(2)}, u32[]{:S(2)}) async-start(bf16[8,16,256]{2,1,0:T(8,128)(2,1)} %bitcast.24), calls=%async_computation.6 | async-start | bytes 131072 | tf_op jit(solution)/shard_map/all_to_all | solution.py:79
where the time goes:
time: 201 us; the launch traced here: 199 us
  blocking collectives  57 us (28%)
  starting transfers between devices  44.1 us (22%)
  waiting for transfers between devices  43.2 us (21%)
  local copies, waits for them, and re-layouts  30.5 us (15%)
  matrix products  15.3 us (8%)
  other arithmetic  7.94 us (4%)
    all_to_all x3, waiting for transfers between devices, from_everyone(): lax.all_to_all(jnp.broadcast_to(shard[None], (peers, *shard.shape)), axis...  30.7 us
    all_to_all x3, starting transfers between devices, from_everyone(): lax.all_to_all(jnp.broadcast_to(shard[None], (peers, *shard.shape)), axis...  28.3 us
    psum x2, blocking collectives, by_axis_2(): return functools.reduce(lax.psum, axes, shard)  24.4 us
    pmax x2, blocking collectives, by_axis(): return functools.reduce(lax.pmax, axes, shard)  23.5 us
    unnamed x22, local copies, waits for them, and re-layouts  22 us
    all_to_all x1, blocking collectives, from_everyone(): lax.all_to_all(jnp.broadcast_to(shard[None], (peers, *shard.shape)), axis...  9.17 us
    all_to_all x1, starting transfers between devices, sent_and_summed(): lax.all_to_all(tiles, axis, split_axis=0, concat_axis=0, tiled=True)  8.44 us
    all_to_all x2, waiting for transfers between devices, sum_at_owner(): lax.all_to_all(tiles, axis, split_axis=0, concat_axis=0, tiled=True)  8.35 us
  transfers between devices with their start and end apart: 6, of which 5 were waited for; matrix products, arithmetic and copies ran while one was open for 12% of the time, Pallas kernels for 0%

commit v1 on v0

v1 whole, which is shorter than its diff:
```python
import functools

import jax
import jax.numpy as jnp
from jax import lax
from jax.experimental import pallas as pl
from jax.experimental.pallas import tpu as pltpu
from jax.sharding import Mesh
from jax.sharding import PartitionSpec as P

KV = ("z", "x")
TP = ("y", "c")
EPS = 1e-06
LANES = 128
F32 = jnp.float32
BF16 = jnp.bfloat16
VMEM = pl.BlockSpec(memory_space=pltpu.VMEM)
HBM = pl.BlockSpec(memory_space=pltpu.HBM)


def local_call(body, name, outs, *args, flops=0, scratch=(), limit=8, far=()):
    cost = pl.CostEstimate(
        flops=flops,
        bytes_accessed=sum(a.size * a.dtype.itemsize for a in args),
        transcendentals=0,
    )
    return pl.pallas_call(
        body,
        name=name,
        out_shape=outs,
        in_specs=[HBM if i in far else VMEM for i in range(len(args))],
        out_specs=jax.tree.map(lambda _: VMEM, outs),
        scratch_shapes=list(scratch),
        cost_estimate=cost,
        compiler_params=pltpu.CompilerParams(vmem_limit_bytes=int(limit * 2**20)),
    )(*args)


def from_peers(shard, axis):
    peers = lax.axis_size(axis)
    return [
        lax.ppermute(shard, axis, [(i, i ^ k) for i in range(peers)])
        for k in range(1, peers)
    ]


def exchanged(tiles, axis):
    return lax.all_to_all(tiles, axis, 0, 0, tiled=True)


def dot(a, b, contract=((1,), (0,))):
    return lax.dot_general(a, b, (contract, ((), ())), preferred_element_type=F32)


def pieces(x):
    hi = x.astype(BF16).astype(F32)
    mid = (x - hi).astype(BF16).astype(F32)
    lo = (x - hi - mid).astype(BF16).astype(F32)
    return hi, mid, lo


def query_body(scaled_ref, squares_ref, w_ref, q_ref):
    q = dot(scaled_ref[...], w_ref[...])
    tiles = q_ref.shape[0] - 1
    for h in range(tiles):
        q_ref[h] = q[:, h * LANES : (h + 1) * LANES]
    q_ref[tiles] = squares_ref[...]


def new_kv_body(scaled_ref, wk_ref, wv_ref, kv_ref):
    rows = scaled_ref.shape[0]
    at = 0
    for w in (wk_ref, wv_ref):
        part = dot(scaled_ref[...], w[...]).astype(BF16)
        for t in range(part.shape[1] // LANES):
            kv_ref[at : at + rows] = part[:, t * LANES : (t + 1) * LANES]
            at += rows


def attention_body(width, q0, q1, q2, q3, kv_ref, k_ref, v_ref, out_ref, inv_ref, q_scr):
    rows, spots, _ = k_ref.shape
    heads = q0.shape[0] - 1
    total_q = (q0[...] + q1[...]) + (q2[...] + q3[...])
    inv = lax.rsqrt(total_q[heads] / width + EPS)
    inv_ref[...] = inv
    for h in range(heads):
        q_scr[:, h, :] = (total_q[h] * inv).astype(BF16).astype(F32) * 0.125
    vecs = 2 * heads
    lane = lax.broadcasted_iota(jnp.int32, (vecs, LANES), 1)
    row = lax.broadcasted_iota(jnp.int32, (vecs, LANES), 0)
    own_half = (lane // 64) == (row // heads)
    wide_lane = lax.broadcasted_iota(jnp.int32, (vecs, spots), 1)
    wide_row = lax.broadcasted_iota(jnp.int32, (vecs, spots), 0)
    own_head = (wide_lane % 2) == ((wide_row % heads) // (heads // 2))

    def step(b, stats):
        q16 = q_scr[b]
        both = jnp.concatenate([q16, q16], axis=0)
        q32 = jnp.where(own_half, both, 0.0).astype(BF16)
        s = dot(q32, k_ref[b], ((1,), (1,)))
        s = jnp.where(own_head, s, -1e30)
        top = jnp.max(s, axis=1, keepdims=True)
        e = jnp.exp(s - top)
        total = jnp.sum(e, axis=1, keepdims=True)
        acc = dot(e.astype(BF16), v_ref[b])
        out_ref[pl.ds(pl.multiple_of(b * vecs, vecs), vecs), :] = acc.astype(BF16)
        here = (lane % 16) == b
        return jnp.where(
            here & (lane < 48), top, jnp.where(here & (lane < 96), total, stats)
        )

    stats = lax.fori_loop(0, rows, step, jnp.zeros((vecs, LANES), F32), unroll=2)
    hi, mid, lo = pieces(stats)
    kind = (lane // 16) % 3
    at = rows * vecs
    out_ref[at : at + vecs] = jnp.where(
        kind == 0, hi, jnp.where(kind == 1, mid, lo)
    ).astype(BF16)
    out_ref[at + vecs :] = kv_ref[...]


def opened_stats(ref, at, vecs):
    p = ref[at : at + vecs].astype(F32)
    whole = p + pltpu.roll(p, LANES - 16, 1) + pltpu.roll(p, LANES - 32, 1)
    return whole, pltpu.roll(whole, LANES - 48, 1)


def merged_stats(refs, at, vecs):
    opened = [opened_stats(r, at, vecs) for r in refs]
    tops = [o[0] for o in opened]
    peak = jnp.maximum(jnp.maximum(tops[0], tops[1]), jnp.maximum(tops[2], tops[3]))
    factors = [jnp.exp(t - peak) for t in tops]
    parts = [f * o[1] for f, o in zip(factors, opened)]
    total = (parts[0] + parts[1]) + (parts[2] + parts[3])
    return peak, total, factors


def weighted(refs, weights, b, start, count, weight_row):
    parts = []
    for r, w in zip(refs, weights):
        block = r[start : start + count].astype(F32)
        parts.append(block * w[weight_row : weight_row + count, b : b + 1])
    return (parts[0] + parts[1]) + (parts[2] + parts[3])


def merge_body(rows, vecs, p0, p1, p2, p3, out_ref):
    refs = (p0, p1, p2, p3)
    at = rows * vecs
    peak, total, factors = merged_stats(refs, at, vecs)
    for b in range(rows):
        acc = weighted(refs, factors, b, b * vecs, vecs, 0)
        out_ref[b * vecs : (b + 1) * vecs] = acc.astype(BF16)
    lane = lax.broadcasted_iota(jnp.int32, (vecs, LANES), 1)
    both = jnp.where(lane < 16, peak, 0.0)
    both = both + pltpu.roll(both, 16, 1) + pltpu.roll(both, 32, 1)
    tot = jnp.where(lane < 16, total, 0.0)
    tot = pltpu.roll(tot, 48, 1) + pltpu.roll(tot, 64, 1) + pltpu.roll(tot, 80, 1)
    hi, mid, lo = pieces(both + tot)
    kind = (lane // 16) % 3
    out_ref[at : at + vecs] = jnp.where(
        kind == 0, hi, jnp.where(kind == 1, mid, lo)
    ).astype(BF16)
    rest = at + vecs
    a, b_, c, d = [r[rest:].astype(F32) for r in refs]
    out_ref[rest:] = ((a + b_) + (c + d)).astype(BF16)


def residual_body(
    rows, vecs, ctx, p0, p1, p2, p3, inv_ref, lam_ref, gain_ref, tok_ref, w_ref,
    res_ref, all_ref, nk_ref, nv_ref, n_scr,
):
    refs = (p0, p1, p2, p3)
    heads = vecs // 2
    at = rows * vecs
    _, total, factors = merged_stats(refs, at, vecs)
    lane = lax.broadcasted_iota(jnp.int32, (vecs, LANES), 1)
    scale = 1.0 / jnp.where(lane < 16, total, 1.0)
    lam = lam_ref[...]
    weights = [
        jnp.concatenate([(f * scale)[:heads], (f * scale)[heads:] * lam], axis=0)
        for f in factors
    ]
    gain = gain_ref[...]
    for b in range(rows):
        first = weighted(refs, weights, b, b * vecs, heads, 0)
        second = weighted(refs, weights, b, b * vecs + heads, heads, heads)
        out = first - second
        mean_sq = jnp.mean(out * out, axis=1, keepdims=True)
        n_scr[:, b, :] = out * lax.rsqrt(mean_sq + 1.0 / ctx) * gain
    normed = jnp.concatenate([n_scr[h].astype(BF16) for h in range(heads)], axis=1)
    res = (tok_ref[...].astype(F32) + dot(normed, w_ref[...])).astype(BF16)
    res_ref[...] = res
    for t in range(all_ref.shape[0]):
        all_ref[t] = res
    rest = at + vecs
    a, b_, c, d = [r[rest:].astype(F32) for r in refs]
    kv = (a + b_) + (c + d)
    inv = inv_ref[...]
    for t in range(2):
        nk_ref[:, t, :] = (kv[t * rows : (t + 1) * rows] * inv).astype(BF16)
        nv_ref[:, t, :] = (kv[(2 + t) * rows : (3 + t) * rows] * inv).astype(BF16)


def diagonal(size):
    a = lax.broadcasted_iota(jnp.int32, (size, size), 0)
    return a == lax.broadcasted_iota(jnp.int32, (size, size), 1)


def up_body(res_ref, gain_ref, w_ref, out_ref):
    groups, rows, width = res_ref.shape
    batch = groups * rows
    res = res_ref[...].reshape(batch, width).astype(F32)
    gained = (res * gain_ref[...]).astype(BF16)
    squares = jnp.sum(res * res, axis=1, keepdims=True)
    line = jnp.sum(jnp.where(diagonal(batch), squares, 0.0), axis=0, keepdims=True)
    hi, mid, lo = pieces(jnp.broadcast_to(line, (16, batch)))
    sub = lax.broadcasted_iota(jnp.int32, (16, batch), 0)
    tail = jnp.where(sub == 0, hi, jnp.where(sub == 1, mid, jnp.where(sub == 2, lo, 0.0)))
    tail = tail.astype(BF16)
    up = dot(gained, w_ref[...])
    for d in range(out_ref.shape[0]):
        out_ref[d, :batch] = up[:, d * LANES : (d + 1) * LANES].astype(BF16)
        out_ref[d, batch:] = tail


def act_body(width, in_ref, out_ref):
    peers, batch, _ = out_ref.shape
    up = in_ref[0, :batch].astype(F32)
    tail = in_ref[0, batch:].astype(F32)
    for p in range(1, peers):
        up = up + in_ref[p, :batch].astype(F32)
        tail = tail + in_ref[p, batch:].astype(F32)
    line = jnp.sum(tail, axis=0, keepdims=True)
    squares = jnp.sum(jnp.where(diagonal(batch), line, 0.0), axis=1, keepdims=True)
    pre = up * lax.rsqrt(squares / width + EPS)
    act = jnp.square(jnp.maximum(pre, 0.0)).astype(BF16)
    for p in range(peers):
        out_ref[p] = act


def down_body(act_ref, w_ref, out_ref):
    peers = act_ref.shape[0]
    acts = jnp.concatenate([act_ref[p] for p in range(peers)], axis=1)
    down = dot(acts, w_ref[...]).astype(BF16)
    out_ref[...] = down.reshape(out_ref.shape)


def final_body(down_ref, res_ref, out_ref):
    total = down_ref[0].astype(F32)
    for t in range(1, down_ref.shape[0]):
        total = total + down_ref[t].astype(F32)
    out_ref[...] = (res_ref[...].astype(F32) + total).astype(BF16)


def shards(
    tokens,
    cache_keys,
    cache_values,
    attn_gain,
    w_query,
    w_key,
    w_value,
    lambdas,
    head_gain,
    w_out,
    mlp_gain,
    w_up,
    w_down,
):
    rows, tok_width = tokens.shape
    n_kv = lax.axis_size(KV)
    n_tp = lax.axis_size(TP)
    width = tok_width * n_kv
    heads = lambdas.shape[0]
    ctx_local, kv_heads, _ = cache_keys.shape[1:]
    ctx = ctx_local * n_kv
    spots = ctx_local * kv_heads
    vecs = 2 * heads
    struct = jax.ShapeDtypeStruct
    batch = rows * n_tp

    tok = tokens.astype(F32)
    scaled = (tok * attn_gain[None, :]).astype(BF16)
    squares = jnp.sum(tok * tok, axis=1, keepdims=True)
    q_part = local_call(
        query_body,
        "query",
        struct((heads + 1, rows, LANES), F32),
        scaled,
        jnp.broadcast_to(squares, (rows, LANES)),
        w_query,
        flops=2 * rows * tok_width * w_query.shape[1],
    )
    kv_part = local_call(
        new_kv_body,
        "new_kv",
        struct((4 * rows, LANES), BF16),
        scaled,
        w_key,
        w_value,
        flops=1 << 33,
    )
    a, b, c = from_peers(q_part, "x")
    q_half = (q_part + a) + (b + c)
    a, b, c = from_peers(q_half, "z")
    packed = rows * vecs + vecs + 4 * rows
    payload, inv_one = local_call(
        functools.partial(attention_body, float(width)),
        "attention",
        (struct((packed, LANES), BF16), struct((rows, LANES), F32)),
        q_half,
        a,
        b,
        c,
        kv_part,
        cache_keys.reshape(rows, spots, LANES),
        cache_values.reshape(rows, spots, LANES),
        flops=4 * rows * vecs * spots * LANES,
        limit=24,
        scratch=(pltpu.VMEM((rows, heads, LANES), F32),),
    )
    payload = local_call(
        functools.partial(merge_body, rows, vecs),
        "merge",
        struct((packed, LANES), BF16),
        payload,
        *from_peers(payload, "x"),
        flops=packed * LANES * 8,
    )
    residual, to_all, new_keys, new_values = local_call(
        functools.partial(residual_body, rows, vecs, float(ctx)),
        "residual",
        (
            struct((rows, tok_width), BF16),
            struct((n_tp, rows, tok_width), BF16),
            struct((rows, kv_heads, LANES), BF16),
            struct((rows, kv_heads, LANES), BF16),
        ),
        payload,
        *from_peers(payload, "z"),
        inv_one,
        jnp.broadcast_to(lambdas[:, None], (heads, LANES)),
        head_gain[None, :],
        tokens,
        w_out,
        flops=2 * rows * heads * LANES * tok_width,
        scratch=(pltpu.VMEM((heads, rows, LANES), F32),),
    )
    everyone = exchanged(to_all, TP)
    up = local_call(
        up_body,
        "up",
        struct((n_kv, batch + 16, LANES), BF16),
        everyone,
        mlp_gain[None, :],
        w_up,
        flops=2 * batch * tok_width * n_kv * LANES,
    )
    acts = local_call(
        functools.partial(act_body, float(width)),
        "act",
        struct((n_kv, batch, LANES), BF16),
        exchanged(up, KV),
        flops=batch * LANES * 40,
    )
    down = local_call(
        down_body,
        "down",
        struct((n_tp, rows, tok_width), BF16),
        exchanged(acts, KV),
        w_down,
        flops=2 * batch * tok_width * n_kv * LANES,
    )
    mixed = local_call(
        final_body,
        "final",
        struct((rows, tok_width), BF16),
        exchanged(down, TP),
        residual,
        flops=rows * tok_width * 10,
    )
    return mixed, new_keys, new_values


def solution(mesh):
    split = Mesh(mesh.devices.reshape(4, 4, 4, 2), ("z", "x", "y", "c"))
    placed = (
        P(TP, KV),
        P(TP, KV, None, None),
        P(TP, KV, None, None),
        P(KV),
        P(KV, None),
        P(KV, None),
        P(KV, None),
        P(),
        P(),
        P(None, KV),
        P(KV),
        P(KV, TP),
        P(TP, KV),
    )
    return jax.shard_map(
        shards,
        mesh=split,
        in_specs=placed,
        out_specs=(P(TP, KV), P(TP, None, None), P(TP, None, None)),
        check_vma=False,
    )
```

time: 201 us -> 107 us (0.53)
  local copies, waits for them, and re-layouts: 30.5 us -> 3.4 us
  starting transfers between devices: 44.1 us -> 17.5 us
  waiting for transfers between devices: 43.2 us -> 18.6 us
  matrix products: 15.3 us -> 0 us
  Pallas kernels: 0 us -> 12.4 us
  other arithmetic: 7.94 us -> 0.85 us
  blocking collectives: 57 us -> 53.4 us
    all_to_all x1 -> x4, blocking collectives: 9.17 us -> 53.4 us  [exchanged(): return lax.all_to_all(tiles, axis, 0, 0, tiled=True)]
    all_to_all x6 -> x0, starting transfers between devices: 44.1 us -> none  [the longest x3 28.3 us: from_everyone(): lax.all_to_all(jnp.broadcast_to(shard[None], (peers, *shard.shape)), axis...]
    all_to_all x6 -> x0, waiting for transfers between devices: 43.2 us -> none  [the longest x3 30.7 us: from_everyone(): lax.all_to_all(jnp.broadcast_to(shard[None], (peers, *shard.shape)), axis...]
    psum x2 -> x0, blocking collectives: 24.4 us -> none  [by_axis_2(): return functools.reduce(lax.psum, axes, shard)]
    pmax x2 -> x0, blocking collectives: 23.5 us -> none  [by_axis(): return functools.reduce(lax.pmax, axes, shard)]
    unnamed x22 -> x28, local copies, waits for them, and re-layouts: 22 us -> 3.26 us
    ppermute x0 -> x12, waiting for transfers between devices: none -> 18.6 us  [from_peers(): lax.ppermute(shard, axis, [(i, i ^ k) for i in range(peers)])]
    ppermute x0 -> x12, starting transfers between devices: none -> 17.5 us  [from_peers(): lax.ppermute(shard, axis, [(i, i ^ k) for i in range(peers)])]
  transfers between devices with their start and end apart: 6 -> 12, of which waited for: 5 -> 8; matrix products, arithmetic and copies ran while one was open for 12% -> 0% of each run, Pallas kernels for 0% -> 0%
where the time goes in v1:
time: 107 us
  blocking collectives  53.4 us (50%)
  waiting for transfers between devices  18.6 us (17%)
  starting transfers between devices  17.5 us (16%)
  Pallas kernels  12.4 us (12%)
  local copies, waits for them, and re-layouts  3.4 us (3%)
    all_to_all x4, blocking collectives, exchanged(): return lax.all_to_all(tiles, axis, 0, 0, tiled=True)  53.4 us
    ppermute x12, waiting for transfers between devices, from_peers(): lax.ppermute(shard, axis, [(i, i ^ k) for i in range(peers)])  18.6 us
    ppermute x12, starting transfers between devices, from_peers(): lax.ppermute(shard, axis, [(i, i ^ k) for i in range(peers)])  17.5 us
    pallas_call x9, Pallas kernels, local_call(): pl.pallas_call(body, name=name, out_shape=outs, in_specs=[HBM if i in far...  12.4 us
    unnamed x28, local copies, waits for them, and re-layouts  3.26 us
  transfers between devices with their start and end apart: 12, of which 8 were waited for; matrix products, arithmetic and copies ran while one was open for 0% of the time, Pallas kernels for 0%

profile of v1, /device:TPU:1, one launch (start us, length us, event | category | flops | bytes accessed | tf_op | source)
XLA Modules:
  0.0 106.9 jit_solution(12533910364371853272)
XLA Ops:
  0.6 0.8 fusion.1
  1.5 1.2 %copy-done.1 = bf16[256,2048]{1,0:T(8,128)(2,1)S(1)} copy-done((bf16[256,2048]{1,0:T(8,128)(2,1)S(1)}, bf16[256,2048]{1,0:T(8,128)(2,1)}, u32[]{:S(2)}) %copy-start.1) | copy-done | bytes 1048600
  3.0 3.3 %collective-permute-start.2 = (f32[17,16,128]{2,1,0:T(8,128)S(1)}, f32[17,16,128]{2,1,0:T(8,128)S(1)}, u32[]{:S(2)}, u32[]{:S(2)}) collective-permute-start(f32[17,16,128]{2,1,0:T(8,128)S(1)} %query.1), channel_id=1, source_target_pairs={{0,24},{8,16},{16,8},{24,0},{1,25},{9,17},{17,9},{25,1},{2,26},{10... | collective-permute-start | bytes 417800 | tf_op jit(solution)/shard_map/ppermute | solution.py:42
  7.0 5.2 %collective-permute-done.2 = f32[17,16,128]{2,1,0:T(8,128)S(1)} collective-permute-done((f32[17,16,128]{2,1,0:T(8,128)S(1)}, f32[17,16,128]{2,1,0:T(8,128)S(1)}, u32[]{:S(2)}, u32[]{:S(2)}) %collective-permute-start.2) | collective-permute-done | bytes 139296 | tf_op jit(solution)/shard_map/ppermute | solution.py:42
  12.2 0.7 collective-permute-done
  12.9 3.9 %collective-permute-start.5 = (f32[17,16,128]{2,1,0:T(8,128)S(1)}, f32[17,16,128]{2,1,0:T(8,128)S(1)}, u32[]{:S(2)}, u32[]{:S(2)}) collective-permute-start(f32[17,16,128]{2,1,0:T(8,128)S(1)} %add_add_fusion.q0), channel_id=1, source_target_pairs={{0,96},{32,64},{64,32},{96,0},{1,97},{33,65},{65,33},{97,1},{2,98}... | collective-permute-start | bytes 417800 | tf_op jit(solution)/shard_map/ppermute | solution.py:42
  16.9 0.7 collective-permute-start.3
  17.5 1.1 copy-done.7
  18.6 0.9 copy-done.8
  19.6 0.7 collective-permute-done.5.q3
  20.4 2.0 %collective-permute-done.4.q2 = f32[17,16,128]{2,1,0:T(8,128)S(1)} collective-permute-done((f32[17,16,128]{2,1,0:T(8,128)S(1)}, f32[17,16,128]{2,1,0:T(8,128)S(1)}, u32[]{:S(2)}, u32[]{:S(2)}) %collective-permute-start.4) | collective-permute-done | bytes 139296 | tf_op jit(solution)/shard_map/ppermute | solution.py:42
  22.5 8.2 %attention.1 = (bf16[608,128]{1,0:T(8,128)(2,1)S(1)}, f32[16,128]{1,0:T(8,128)S(1)}) custom-call(f32[17,16,128]{2,1,0:T(8,128)S(1)} %add_add_fusion.q0, f32[17,16,128]{2,1,0:T(8,128)S(1)} %collective-permute-done.3.q1, f32[17,16,128]{2,1,0:T(8,128)S(1)} %collective-permute-done.4.q2, f32[17,16,128]{2,1,0:T(8,128)S(1)} %collective-permute-done.5.q3, ...), custom_call_target="tpu_custom_call" | custom-call | flops 536870912 | bytes 17350656 | tf_op jit(solution)/shard_map/attention/pallas_call | solution.py:27
  30.7 3.1 %collective-permute-start.8 = (bf16[608,128]{1,0:T(8,128)(2,1)S(1)}, bf16[608,128]{1,0:T(8,128)(2,1)S(1)}, u32[]{:S(2)}, u32[]{:S(2)}) collective-permute-start(bf16[608,128]{1,0:T(8,128)(2,1)S(1)} %get-tuple-element.9.p0), channel_id=1, source_target_pairs={{0,24},{8,16},{16,8},{24,0},{1,25},{9,17},{17,9},{25,1},{2,26},{10... | collective-permute-start | bytes 466952 | tf_op jit(solution)/shard_map/ppermute | solution.py:42
  34.5 3.2 %collective-permute-done.8.p3 = bf16[608,128]{1,0:T(8,128)(2,1)S(1)} collective-permute-done((bf16[608,128]{1,0:T(8,128)(2,1)S(1)}, bf16[608,128]{1,0:T(8,128)(2,1)S(1)}, u32[]{:S(2)}, u32[]{:S(2)}) %collective-permute-start.8) | collective-permute-done | bytes 155680 | tf_op jit(solution)/shard_map/ppermute | solution.py:42
  37.7 1.8 %collective-permute-done.7.p2 = bf16[608,128]{1,0:T(8,128)(2,1)S(1)} collective-permute-done((bf16[608,128]{1,0:T(8,128)(2,1)S(1)}, bf16[608,128]{1,0:T(8,128)(2,1)S(1)}, u32[]{:S(2)}, u32[]{:S(2)}) %collective-permute-start.7) | collective-permute-done | bytes 155680 | tf_op jit(solution)/shard_map/ppermute | solution.py:42
  40.0 4.4 %collective-permute-start.11 = (bf16[608,128]{1,0:T(8,128)(2,1)S(1)}, bf16[608,128]{1,0:T(8,128)(2,1)S(1)}, u32[]{:S(2)}, u32[]{:S(2)}) collective-permute-start(bf16[608,128]{1,0:T(8,128)(2,1)S(1)} %merge.1.p0), channel_id=1, source_target_pairs={{0,96},{32,64},{64,32},{96,0},{1,97},{33,65},{65,33},{97,1},{2,98}... | collective-permute-start | bytes 466952 | tf_op jit(solution)/shard_map/ppermute | solution.py:42
  44.4 0.7 collective-permute-start.9
  45.0 3.2 %collective-permute-done.11.p3 = bf16[608,128]{1,0:T(8,128)(2,1)S(1)} collective-permute-done((bf16[608,128]{1,0:T(8,128)(2,1)S(1)}, bf16[608,128]{1,0:T(8,128)(2,1)S(1)}, u32[]{:S(2)}, u32[]{:S(2)}) %collective-permute-start.11) | collective-permute-done | bytes 155680 | tf_op jit(solution)/shard_map/ppermute | solution.py:42
  48.2 1.8 %collective-permute-done.10.p2 = bf16[608,128]{1,0:T(8,128)(2,1)S(1)} collective-permute-done((bf16[608,128]{1,0:T(8,128)(2,1)S(1)}, bf16[608,128]{1,0:T(8,128)(2,1)S(1)}, u32[]{:S(2)}, u32[]{:S(2)}) %collective-permute-start.10) | collective-permute-done | bytes 155680 | tf_op jit(solution)/shard_map/ppermute | solution.py:42
  50.1 2.0 %residual.1 = (bf16[16,256]{1,0:T(8,128)(2,1)S(1)}, bf16[8,16,256]{2,1,0:T(8,128)(2,1)S(1)}, bf16[16,2,128]{2,1,0:T(2,128)(2,1)}, bf16[16,2,128]{2,1,0:T(2,128)(2,1)}) custom-call(bf16[608,128]{1,0:T(8,128)(2,1)S(1)} %merge.1.p0, bf16[608,128]{1,0:T(8,128)(2,1)S(1)} %collective-permute-done.9.p1, bf16[608,128]{1,0:T(8,128)(2,1)S(1)} %collective-permute-done.10.p2, ...), custom_call_target="tpu_custom_call" | custom-call | flops 16777216 | bytes 1696256 | tf_op jit(solution)/shard_map/residual/pallas_call | solution.py:27
  52.1 13.5 %all_to_all.20.res_ref = bf16[8,16,256]{2,1,0:T(8,128)(2,1)S(1)} all-to-all(bf16[8,16,256]{2,1,0:T(8,128)(2,1)S(1)} %get-tuple-element.11), channel_id=1, replica_groups=mesh['z'=4,'x'=4,'y'=4,'c'=2] {'y','c'}, dimensions={0} | all-to-all | bytes 131072 | tf_op jit(solution)/shard_map/all_to_all | solution.py:48
  66.0 17.2 %all_to_all.21.in_ref = bf16[16,144,128]{2,1,0:T(8,128)(2,1)S(1)} all-to-all(bf16[16,144,128]{2,1,0:T(8,128)(2,1)S(1)} %up.1), channel_id=1, replica_groups=mesh['z'=4,'x'=4,'y'=4,'c'=2] {'z','x'}, dimensions={0} | all-to-all | bytes 1179648 | tf_op jit(solution)/shard_map/all_to_all | solution.py:48
  83.3 12.3 %all_to_all.22.act_ref = bf16[16,128,128]{2,1,0:T(8,128)(2,1)S(1)} all-to-all(bf16[16,128,128]{2,1,0:T(8,128)(2,1)S(1)} %act.1), channel_id=1, replica_groups=mesh['z'=4,'x'=4,'y'=4,'c'=2] {'z','x'}, dimensions={0} | all-to-all | bytes 1048576 | tf_op jit(solution)/shard_map/all_to_all | solution.py:48
  96.0 10.3 %all_to_all.23.down_ref = bf16[8,16,256]{2,1,0:T(8,128)(2,1)S(1)} all-to-all(bf16[8,16,256]{2,1,0:T(8,128)(2,1)S(1)} %down.1), channel_id=1, replica_groups=mesh['z'=4,'x'=4,'y'=4,'c'=2] {'y','c'}, dimensions={0} | all-to-all | bytes 131072 | tf_op jit(solution)/shard_map/all_to_all | solution.py:48
  (47 shorter events, 3.9 us)
Async XLA Ops:
  1.5 1.2 %copy-start.1 = (bf16[256,2048]{1,0:T(8,128)(2,1)S(1)}, bf16[256,2048]{1,0:T(8,128)(2,1)}, u32[]{:S(2)}) copy-start(bf16[256,2048]{1,0:T(8,128)(2,1)} %w_ref.4) | copy-start | bytes 3145732
  3.0 9.2 %collective-permute-start.2 = (f32[17,16,128]{2,1,0:T(8,128)S(1)}, f32[17,16,128]{2,1,0:T(8,128)S(1)}, u32[]{:S(2)}, u32[]{:S(2)}) collective-permute-start(f32[17,16,128]{2,1,0:T(8,128)S(1)} %query.1), channel_id=1, source_target_pairs={{0,24},{8,16},{16,8},{24,0},{1,25},{9,17},{17,9},{25,1},{2,26},{10... | collective-permute-start | bytes 417800 | tf_op jit(solution)/shard_map/ppermute | solution.py:42
  6.3 5.9 %collective-permute-start.1 = (f32[17,16,128]{2,1,0:T(8,128)S(1)}, f32[17,16,128]{2,1,0:T(8,128)S(1)}, u32[]{:S(2)}, u32[]{:S(2)}) collective-permute-start(f32[17,16,128]{2,1,0:T(8,128)S(1)} %query.1), channel_id=1, source_target_pairs={{0,16},{8,24},{16,0},{24,8},{1,17},{9,25},{17,1},{25,9},{2,18},{10... | collective-permute-start | bytes 417800 | tf_op jit(solution)/shard_map/ppermute | solution.py:42
  6.8 6.0 %collective-permute-start = (f32[17,16,128]{2,1,0:T(8,128)S(1)}, f32[17,16,128]{2,1,0:T(8,128)S(1)}, u32[]{:S(2)}, u32[]{:S(2)}) collective-permute-start(f32[17,16,128]{2,1,0:T(8,128)S(1)} %query.1), channel_id=1, source_target_pairs={{0,8},{8,0},{16,24},{24,16},{1,9},{9,1},{17,25},{25,17},{2,10},{10... | collective-permute-start | bytes 417800 | tf_op jit(solution)/shard_map/ppermute | solution.py:42
  12.8 9.5 %slice-start = ((s8[8388608]{0:T(1024)(128)(4,1)}), s8[4194304]{0:T(1024)(128)(4,1)S(1)}, s32[]{:S(2)}) async-start(s8[8388608]{0:T(1024)(128)(4,1)} %bitcast.4), calls=%async_computation.4 | async-start | bytes 8388608
  12.9 9.5 %slice-start.2 = ((s8[8388608]{0:T(1024)(128)(4,1)}), s8[4194304]{0:T(1024)(128)(4,1)S(1)}, s32[]{:S(2)}) async-start(s8[8388608]{0:T(1024)(128)(4,1)} %bitcast.7), calls=%async_computation.6 | async-start | bytes 8388608
  12.9 9.5 %slice-start.1 = ((s8[8388608]{0:T(1024)(128)(4,1)}), s8[4194304]{0:T(1024)(128)(4,1)S(1)}, s32[]{:S(2)}) async-start(s8[8388608]{0:T(1024)(128)(4,1)} %bitcast.4), calls=%async_computation.5 | async-start | bytes 8388608
  12.9 9.5 %slice-start.3 = ((s8[8388608]{0:T(1024)(128)(4,1)}), s8[4194304]{0:T(1024)(128)(4,1)S(1)}, s32[]{:S(2)}) async-start(s8[8388608]{0:T(1024)(128)(4,1)} %bitcast.7), calls=%async_computation.7 | async-start | bytes 8388608
  12.9 7.4 %collective-permute-start.5 = (f32[17,16,128]{2,1,0:T(8,128)S(1)}, f32[17,16,128]{2,1,0:T(8,128)S(1)}, u32[]{:S(2)}, u32[]{:S(2)}) collective-permute-start(f32[17,16,128]{2,1,0:T(8,128)S(1)} %add_add_fusion.q0), channel_id=1, source_target_pairs={{0,96},{32,64},{64,32},{96,0},{1,97},{33,65},{65,33},{97,1},{2,98}... | collective-permute-start | bytes 417800 | tf_op jit(solution)/shard_map/ppermute | solution.py:42
  16.9 5.5 %collective-permute-start.4 = (f32[17,16,128]{2,1,0:T(8,128)S(1)}, f32[17,16,128]{2,1,0:T(8,128)S(1)}, u32[]{:S(2)}, u32[]{:S(2)}) collective-permute-start(f32[17,16,128]{2,1,0:T(8,128)S(1)} %add_add_fusion.q0), channel_id=1, source_target_pairs={{0,64},{32,96},{64,0},{96,32},{1,65},{33,97},{65,1},{97,33},{2,66}... | collective-permute-start | bytes 417800 | tf_op jit(solution)/shard_map/ppermute | solution.py:42
  16.9 5.5 %collective-permute-start.3 = (f32[17,16,128]{2,1,0:T(8,128)S(1)}, f32[17,16,128]{2,1,0:T(8,128)S(1)}, u32[]{:S(2)}, u32[]{:S(2)}) collective-permute-start(f32[17,16,128]{2,1,0:T(8,128)S(1)} %add_add_fusion.q0), channel_id=1, source_target_pairs={{0,32},{32,0},{64,96},{96,64},{1,33},{33,1},{65,97},{97,65},{2,34}... | collective-permute-start | bytes 417800 | tf_op jit(solution)/shard_map/ppermute | solution.py:42
  22.4 27.6 %copy-start.9 = (f32[16]{0:T(128)S(1)}, f32[16]{0:T(128)}, u32[]{:S(2)}) copy-start(f32[16]{0:T(128)} %param.20) | copy-start | bytes 196
  22.4 27.7 %copy-start = (bf16[2048,256]{1,0:T(8,128)(2,1)S(1)}, bf16[2048,256]{1,0:T(8,128)(2,1)}, u32[]{:S(2)}) copy-start(bf16[2048,256]{1,0:T(8,128)(2,1)} %w_ref.5) | copy-start | bytes 3145732
  22.5 27.7 %copy-start.4 = (bf16[16,256]{1,0:T(8,128)(2,1)S(1)}, bf16[16,256]{1,0:T(8,128)(2,1)}, u32[]{:S(2)}) copy-start(bf16[16,256]{1,0:T(8,128)(2,1)} %tok_ref.1) | copy-start | bytes 24580
  22.5 27.7 %copy-start.6 = (f32[128]{0:T(128)S(1)}, f32[128]{0:T(128)}, u32[]{:S(2)}) copy-start(f32[128]{0:T(128)} %param.21) | copy-start | bytes 1540
  22.5 43.2 %copy-start.2 = (bf16[256,2048]{1,0:T(8,128)(2,1)S(1)}, bf16[256,2048]{1,0:T(8,128)(2,1)}, u32[]{:S(2)}) copy-start(bf16[256,2048]{1,0:T(8,128)(2,1)} %w_ref.6) | copy-start | bytes 3145732
  22.5 43.2 %copy-start.5 = (f32[256]{0:T(256)S(1)}, f32[256]{0:T(256)}, u32[]{:S(2)}) copy-start(f32[256]{0:T(256)} %param.23) | copy-start | bytes 3076
  22.5 73.2 %copy-start.3 = (bf16[2048,256]{1,0:T(8,128)(2,1)S(1)}, bf16[2048,256]{1,0:T(8,128)(2,1)}, u32[]{:S(2)}) copy-start(bf16[2048,256]{1,0:T(8,128)(2,1)} %w_ref.7) | copy-start | bytes 3145732
  30.7 7.0 %collective-permute-start.8 = (bf16[608,128]{1,0:T(8,128)(2,1)S(1)}, bf16[608,128]{1,0:T(8,128)(2,1)S(1)}, u32[]{:S(2)}, u32[]{:S(2)}) collective-permute-start(bf16[608,128]{1,0:T(8,128)(2,1)S(1)} %get-tuple-element.9.p0), channel_id=1, source_target_pairs={{0,24},{8,16},{16,8},{24,0},{1,25},{9,17},{17,9},{25,1},{2,26},{10... | collective-permute-start | bytes 466952 | tf_op jit(solution)/shard_map/ppermute | solution.py:42
  33.8 5.7 %collective-permute-start.7 = (bf16[608,128]{1,0:T(8,128)(2,1)S(1)}, bf16[608,128]{1,0:T(8,128)(2,1)S(1)}, u32[]{:S(2)}, u32[]{:S(2)}) collective-permute-start(bf16[608,128]{1,0:T(8,128)(2,1)S(1)} %get-tuple-element.9.p0), channel_id=1, source_target_pairs={{0,16},{8,24},{16,0},{24,8},{1,17},{9,25},{17,1},{25,9},{2,18},{10... | collective-permute-start | bytes 466952 | tf_op jit(solution)/shard_map/ppermute | solution.py:42
  34.0 5.5 %collective-permute-start.6 = (bf16[608,128]{1,0:T(8,128)(2,1)S(1)}, bf16[608,128]{1,0:T(8,128)(2,1)S(1)}, u32[]{:S(2)}, u32[]{:S(2)}) collective-permute-start(bf16[608,128]{1,0:T(8,128)(2,1)S(1)} %get-tuple-element.9.p0), channel_id=1, source_target_pairs={{0,8},{8,0},{16,24},{24,16},{1,9},{9,1},{17,25},{25,17},{2,10},{10... | collective-permute-start | bytes 466952 | tf_op jit(solution)/shard_map/ppermute | solution.py:42
  40.0 8.2 %collective-permute-start.11 = (bf16[608,128]{1,0:T(8,128)(2,1)S(1)}, bf16[608,128]{1,0:T(8,128)(2,1)S(1)}, u32[]{:S(2)}, u32[]{:S(2)}) collective-permute-start(bf16[608,128]{1,0:T(8,128)(2,1)S(1)} %merge.1.p0), channel_id=1, source_target_pairs={{0,96},{32,64},{64,32},{96,0},{1,97},{33,65},{65,33},{97,1},{2,98}... | collective-permute-start | bytes 466952 | tf_op jit(solution)/shard_map/ppermute | solution.py:42
  44.4 5.7 %collective-permute-start.10 = (bf16[608,128]{1,0:T(8,128)(2,1)S(1)}, bf16[608,128]{1,0:T(8,128)(2,1)S(1)}, u32[]{:S(2)}, u32[]{:S(2)}) collective-permute-start(bf16[608,128]{1,0:T(8,128)(2,1)S(1)} %merge.1.p0), channel_id=1, source_target_pairs={{0,64},{32,96},{64,0},{96,32},{1,65},{33,97},{65,1},{97,33},{2,66}... | collective-permute-start | bytes 466952 | tf_op jit(solution)/shard_map/ppermute | solution.py:42
  44.4 5.7 %collective-permute-start.9 = (bf16[608,128]{1,0:T(8,128)(2,1)S(1)}, bf16[608,128]{1,0:T(8,128)(2,1)S(1)}, u32[]{:S(2)}, u32[]{:S(2)}) collective-permute-start(bf16[608,128]{1,0:T(8,128)(2,1)S(1)} %merge.1.p0), channel_id=1, source_target_pairs={{0,32},{32,0},{64,96},{96,64},{1,33},{33,1},{65,97},{97,65},{2,34}... | collective-permute-start | bytes 466952 | tf_op jit(solution)/shard_map/ppermute | solution.py:42
  (2 other events, 2.0 us)

commit v2 on v1

--- a/solution.py
+++ b/solution.py
@@ -77,7 +77,7 @@
             at += rows
 
 
-def attention_body(width, q0, q1, q2, q3, kv_ref, k_ref, v_ref, out_ref, inv_ref, q_scr):
+def attention_body(width, q0, q1, q2, q3, kv_ref, k_ref, v_ref, out_ref, inv_ref, q_scr, s_scr):
     rows, spots, _ = k_ref.shape
     heads = q0.shape[0] - 1
     total_q = (q0[...] + q1[...]) + (q2[...] + q3[...])
@@ -93,11 +93,13 @@
     wide_row = lax.broadcasted_iota(jnp.int32, (vecs, spots), 0)
     own_head = (wide_lane % 2) == ((wide_row % heads) // (heads // 2))
 
-    def step(b, stats):
+    def scores(b):
         q16 = q_scr[b]
         both = jnp.concatenate([q16, q16], axis=0)
         q32 = jnp.where(own_half, both, 0.0).astype(BF16)
-        s = dot(q32, k_ref[b], ((1,), (1,)))
+        return dot(q32, k_ref[b], ((1,), (1,)))
+
+    def finish(b, s, stats):
         s = jnp.where(own_head, s, -1e30)
         top = jnp.max(s, axis=1, keepdims=True)
         e = jnp.exp(s - top)
@@ -109,7 +111,19 @@
             here & (lane < 48), top, jnp.where(here & (lane < 96), total, stats)
         )
 
-    stats = lax.fori_loop(0, rows, step, jnp.zeros((vecs, LANES), F32), unroll=2)
+    deep = 4
+    s_scr[0] = scores(0)
+
+    def step(i, stats):
+        for u in range(deep):
+            b = i * deep + u
+            current = s_scr[u % 2]
+            following = scores(jnp.minimum(b + 1, rows - 1))
+            stats = finish(b, current, stats)
+            s_scr[(u + 1) % 2] = following
+        return stats
+
+    stats = lax.fori_loop(0, rows // deep, step, jnp.zeros((vecs, LANES), F32))
     hi, mid, lo = pieces(stats)
     kind = (lane // 16) % 3
     at = rows * vecs
@@ -317,7 +331,10 @@
         cache_values.reshape(rows, spots, LANES),
         flops=4 * rows * vecs * spots * LANES,
         limit=24,
-        scratch=(pltpu.VMEM((rows, heads, LANES), F32),),
+        scratch=(
+            pltpu.VMEM((rows, heads, LANES), F32),
+            pltpu.VMEM((2, vecs, spots), F32),
+        ),
     )
     payload = local_call(
         functools.partial(merge_body, rows, vecs),

time: 107 us -> 104 us (0.972)
  Pallas kernels: 12.4 us -> 9.29 us
    pallas_call x9, Pallas kernels: 12.4 us -> 9.29 us  [local_call(): pl.pallas_call(body, name=name, out_shape=outs, in_specs=[HBM if i in far...]
where the time goes in v2:
time: 104 us
  blocking collectives  53.3 us (51%)
  waiting for transfers between devices  18.6 us (18%)
  starting transfers between devices  17.5 us (17%)
  Pallas kernels  9.29 us (9%)
  local copies, waits for them, and re-layouts  3.4 us (3%)
    all_to_all x4, blocking collectives, exchanged(): return lax.all_to_all(tiles, axis, 0, 0, tiled=True)  53.3 us
    ppermute x12, waiting for transfers between devices, from_peers(): lax.ppermute(shard, axis, [(i, i ^ k) for i in range(peers)])  18.6 us
    ppermute x12, starting transfers between devices, from_peers(): lax.ppermute(shard, axis, [(i, i ^ k) for i in range(peers)])  17.5 us
    pallas_call x9, Pallas kernels, local_call(): pl.pallas_call(body, name=name, out_shape=outs, in_specs=[HBM if i in far...  9.29 us
    unnamed x28, local copies, waits for them, and re-layouts  3.26 us
  transfers between devices with their start and end apart: 12, of which 8 were waited for; matrix products, arithmetic and copies ran while one was open for 0% of the time, Pallas kernels for 0%

profile of v2, /device:TPU:1, one launch (start us, length us, event | category | flops | bytes accessed | tf_op | source)
XLA Modules:
  0.0 103.8 jit_solution(1954772254999751185)
XLA Ops:
  0.6 0.8 fusion.1
  1.5 1.2 %copy-done.1 = bf16[256,2048]{1,0:T(8,128)(2,1)S(1)} copy-done((bf16[256,2048]{1,0:T(8,128)(2,1)S(1)}, bf16[256,2048]{1,0:T(8,128)(2,1)}, u32[]{:S(2)}) %copy-start.1) | copy-done | bytes 1048600
  3.0 3.3 %collective-permute-start.2 = (f32[17,16,128]{2,1,0:T(8,128)S(1)}, f32[17,16,128]{2,1,0:T(8,128)S(1)}, u32[]{:S(2)}, u32[]{:S(2)}) collective-permute-start(f32[17,16,128]{2,1,0:T(8,128)S(1)} %query.1), channel_id=1, source_target_pairs={{0,24},{8,16},{16,8},{24,0},{1,25},{9,17},{17,9},{25,1},{2,26},{10... | collective-permute-start | bytes 417800 | tf_op jit(solution)/shard_map/ppermute | solution.py:42
  7.0 5.2 %collective-permute-done.2 = f32[17,16,128]{2,1,0:T(8,128)S(1)} collective-permute-done((f32[17,16,128]{2,1,0:T(8,128)S(1)}, f32[17,16,128]{2,1,0:T(8,128)S(1)}, u32[]{:S(2)}, u32[]{:S(2)}) %collective-permute-start.2) | collective-permute-done | bytes 139296 | tf_op jit(solution)/shard_map/ppermute | solution.py:42
  12.2 0.7 collective-permute-done
  12.9 3.9 %collective-permute-start.5 = (f32[17,16,128]{2,1,0:T(8,128)S(1)}, f32[17,16,128]{2,1,0:T(8,128)S(1)}, u32[]{:S(2)}, u32[]{:S(2)}) collective-permute-start(f32[17,16,128]{2,1,0:T(8,128)S(1)} %add_add_fusion.q0), channel_id=1, source_target_pairs={{0,96},{32,64},{64,32},{96,0},{1,97},{33,65},{65,33},{97,1},{2,98}... | collective-permute-start | bytes 417800 | tf_op jit(solution)/shard_map/ppermute | solution.py:42
  16.9 0.7 collective-permute-start.3
  17.5 1.1 %copy-done.7 = bf16[256,256]{1,0:T(8,128)(2,1)S(1)} copy-done((bf16[256,256]{1,0:T(8,128)(2,1)S(1)}, bf16[256,256]{1,0:T(8,128)(2,1)}, u32[]{:S(2)}) %copy-start.7) | copy-done | bytes 131096
  18.6 0.9 copy-done.8
  19.6 0.7 collective-permute-done.5.q3
  20.4 2.0 %collective-permute-done.4.q2 = f32[17,16,128]{2,1,0:T(8,128)S(1)} collective-permute-done((f32[17,16,128]{2,1,0:T(8,128)S(1)}, f32[17,16,128]{2,1,0:T(8,128)S(1)}, u32[]{:S(2)}, u32[]{:S(2)}) %collective-permute-start.4) | collective-permute-done | bytes 139296 | tf_op jit(solution)/shard_map/ppermute | solution.py:42
  22.5 5.1 %attention.1 = (bf16[608,128]{1,0:T(8,128)(2,1)S(1)}, f32[16,128]{1,0:T(8,128)S(1)}) custom-call(f32[17,16,128]{2,1,0:T(8,128)S(1)} %add_add_fusion.q0, f32[17,16,128]{2,1,0:T(8,128)S(1)} %collective-permute-done.3.q1, f32[17,16,128]{2,1,0:T(8,128)S(1)} %collective-permute-done.4.q2, f32[17,16,128]{2,1,0:T(8,128)S(1)} %collective-permute-done.5.q3, ...), custom_call_target="tpu_custom_call" | custom-call | flops 536870912 | bytes 17350656 | tf_op jit(solution)/shard_map/attention/pallas_call | solution.py:27
  27.6 3.1 %collective-permute-start.8 = (bf16[608,128]{1,0:T(8,128)(2,1)S(1)}, bf16[608,128]{1,0:T(8,128)(2,1)S(1)}, u32[]{:S(2)}, u32[]{:S(2)}) collective-permute-start(bf16[608,128]{1,0:T(8,128)(2,1)S(1)} %get-tuple-element.9.p0), channel_id=1, source_target_pairs={{0,24},{8,16},{16,8},{24,0},{1,25},{9,17},{17,9},{25,1},{2,26},{10... | collective-permute-start | bytes 466952 | tf_op jit(solution)/shard_map/ppermute | solution.py:42
  31.4 3.2 %collective-permute-done.8.p3 = bf16[608,128]{1,0:T(8,128)(2,1)S(1)} collective-permute-done((bf16[608,128]{1,0:T(8,128)(2,1)S(1)}, bf16[608,128]{1,0:T(8,128)(2,1)S(1)}, u32[]{:S(2)}, u32[]{:S(2)}) %collective-permute-start.8) | collective-permute-done | bytes 155680 | tf_op jit(solution)/shard_map/ppermute | solution.py:42
  34.6 1.8 %collective-permute-done.7.p2 = bf16[608,128]{1,0:T(8,128)(2,1)S(1)} collective-permute-done((bf16[608,128]{1,0:T(8,128)(2,1)S(1)}, bf16[608,128]{1,0:T(8,128)(2,1)S(1)}, u32[]{:S(2)}, u32[]{:S(2)}) %collective-permute-start.7) | collective-permute-done | bytes 155680 | tf_op jit(solution)/shard_map/ppermute | solution.py:42
  36.9 4.4 %collective-permute-start.11 = (bf16[608,128]{1,0:T(8,128)(2,1)S(1)}, bf16[608,128]{1,0:T(8,128)(2,1)S(1)}, u32[]{:S(2)}, u32[]{:S(2)}) collective-permute-start(bf16[608,128]{1,0:T(8,128)(2,1)S(1)} %merge.1.p0), channel_id=1, source_target_pairs={{0,96},{32,64},{64,32},{96,0},{1,97},{33,65},{65,33},{97,1},{2,98}... | collective-permute-start | bytes 466952 | tf_op jit(solution)/shard_map/ppermute | solution.py:42
  41.3 0.7 collective-permute-start.9
  41.9 3.2 %collective-permute-done.11.p3 = bf16[608,128]{1,0:T(8,128)(2,1)S(1)} collective-permute-done((bf16[608,128]{1,0:T(8,128)(2,1)S(1)}, bf16[608,128]{1,0:T(8,128)(2,1)S(1)}, u32[]{:S(2)}, u32[]{:S(2)}) %collective-permute-start.11) | collective-permute-done | bytes 155680 | tf_op jit(solution)/shard_map/ppermute | solution.py:42
  45.1 1.8 %collective-permute-done.10.p2 = bf16[608,128]{1,0:T(8,128)(2,1)S(1)} collective-permute-done((bf16[608,128]{1,0:T(8,128)(2,1)S(1)}, bf16[608,128]{1,0:T(8,128)(2,1)S(1)}, u32[]{:S(2)}, u32[]{:S(2)}) %collective-permute-start.10) | collective-permute-done | bytes 155680 | tf_op jit(solution)/shard_map/ppermute | solution.py:42
  47.1 2.0 %residual.1 = (bf16[16,256]{1,0:T(8,128)(2,1)S(1)}, bf16[8,16,256]{2,1,0:T(8,128)(2,1)S(1)}, bf16[16,2,128]{2,1,0:T(2,128)(2,1)}, bf16[16,2,128]{2,1,0:T(2,128)(2,1)}) custom-call(bf16[608,128]{1,0:T(8,128)(2,1)S(1)} %merge.1.p0, bf16[608,128]{1,0:T(8,128)(2,1)S(1)} %collective-permute-done.9.p1, bf16[608,128]{1,0:T(8,128)(2,1)S(1)} %collective-permute-done.10.p2, ...), custom_call_target="tpu_custom_call" | custom-call | flops 16777216 | bytes 1696256 | tf_op jit(solution)/shard_map/residual/pallas_call | solution.py:27
  49.0 13.5 %all_to_all.20.res_ref = bf16[8,16,256]{2,1,0:T(8,128)(2,1)S(1)} all-to-all(bf16[8,16,256]{2,1,0:T(8,128)(2,1)S(1)} %get-tuple-element.11), channel_id=1, replica_groups=mesh['z'=4,'x'=4,'y'=4,'c'=2] {'y','c'}, dimensions={0} | all-to-all | bytes 131072 | tf_op jit(solution)/shard_map/all_to_all | solution.py:48
  62.9 17.2 %all_to_all.21.in_ref = bf16[16,144,128]{2,1,0:T(8,128)(2,1)S(1)} all-to-all(bf16[16,144,128]{2,1,0:T(8,128)(2,1)S(1)} %up.1), channel_id=1, replica_groups=mesh['z'=4,'x'=4,'y'=4,'c'=2] {'z','x'}, dimensions={0} | all-to-all | bytes 1179648 | tf_op jit(solution)/shard_map/all_to_all | solution.py:48
  80.2 12.3 %all_to_all.22.act_ref = bf16[16,128,128]{2,1,0:T(8,128)(2,1)S(1)} all-to-all(bf16[16,128,128]{2,1,0:T(8,128)(2,1)S(1)} %act.1), channel_id=1, replica_groups=mesh['z'=4,'x'=4,'y'=4,'c'=2] {'z','x'}, dimensions={0} | all-to-all | bytes 1048576 | tf_op jit(solution)/shard_map/all_to_all | solution.py:48
  92.9 10.3 %all_to_all.23.down_ref = bf16[8,16,256]{2,1,0:T(8,128)(2,1)S(1)} all-to-all(bf16[8,16,256]{2,1,0:T(8,128)(2,1)S(1)} %down.1), channel_id=1, replica_groups=mesh['z'=4,'x'=4,'y'=4,'c'=2] {'y','c'}, dimensions={0} | all-to-all | bytes 131072 | tf_op jit(solution)/shard_map/all_to_all | solution.py:48
  (47 shorter events, 3.9 us)
Async XLA Ops:
  1.5 1.2 %copy-start.1 = (bf16[256,2048]{1,0:T(8,128)(2,1)S(1)}, bf16[256,2048]{1,0:T(8,128)(2,1)}, u32[]{:S(2)}) copy-start(bf16[256,2048]{1,0:T(8,128)(2,1)} %w_ref.4) | copy-start | bytes 3145732
  3.0 9.2 %collective-permute-start.2 = (f32[17,16,128]{2,1,0:T(8,128)S(1)}, f32[17,16,128]{2,1,0:T(8,128)S(1)}, u32[]{:S(2)}, u32[]{:S(2)}) collective-permute-start(f32[17,16,128]{2,1,0:T(8,128)S(1)} %query.1), channel_id=1, source_target_pairs={{0,24},{8,16},{16,8},{24,0},{1,25},{9,17},{17,9},{25,1},{2,26},{10... | collective-permute-start | bytes 417800 | tf_op jit(solution)/shard_map/ppermute | solution.py:42
  6.3 5.9 %collective-permute-start.1 = (f32[17,16,128]{2,1,0:T(8,128)S(1)}, f32[17,16,128]{2,1,0:T(8,128)S(1)}, u32[]{:S(2)}, u32[]{:S(2)}) collective-permute-start(f32[17,16,128]{2,1,0:T(8,128)S(1)} %query.1), channel_id=1, source_target_pairs={{0,16},{8,24},{16,0},{24,8},{1,17},{9,25},{17,1},{25,9},{2,18},{10... | collective-permute-start | bytes 417800 | tf_op jit(solution)/shard_map/ppermute | solution.py:42
  6.8 6.0 %collective-permute-start = (f32[17,16,128]{2,1,0:T(8,128)S(1)}, f32[17,16,128]{2,1,0:T(8,128)S(1)}, u32[]{:S(2)}, u32[]{:S(2)}) collective-permute-start(f32[17,16,128]{2,1,0:T(8,128)S(1)} %query.1), channel_id=1, source_target_pairs={{0,8},{8,0},{16,24},{24,16},{1,9},{9,1},{17,25},{25,17},{2,10},{10... | collective-permute-start | bytes 417800 | tf_op jit(solution)/shard_map/ppermute | solution.py:42
  12.8 9.5 %slice-start = ((s8[8388608]{0:T(1024)(128)(4,1)}), s8[4194304]{0:T(1024)(128)(4,1)S(1)}, s32[]{:S(2)}) async-start(s8[8388608]{0:T(1024)(128)(4,1)} %bitcast.4), calls=%async_computation.4 | async-start | bytes 8388608
  12.9 9.5 %slice-start.2 = ((s8[8388608]{0:T(1024)(128)(4,1)}), s8[4194304]{0:T(1024)(128)(4,1)S(1)}, s32[]{:S(2)}) async-start(s8[8388608]{0:T(1024)(128)(4,1)} %bitcast.7), calls=%async_computation.6 | async-start | bytes 8388608
  12.9 9.5 %slice-start.1 = ((s8[8388608]{0:T(1024)(128)(4,1)}), s8[4194304]{0:T(1024)(128)(4,1)S(1)}, s32[]{:S(2)}) async-start(s8[8388608]{0:T(1024)(128)(4,1)} %bitcast.4), calls=%async_computation.5 | async-start | bytes 8388608
  12.9 9.5 %slice-start.3 = ((s8[8388608]{0:T(1024)(128)(4,1)}), s8[4194304]{0:T(1024)(128)(4,1)S(1)}, s32[]{:S(2)}) async-start(s8[8388608]{0:T(1024)(128)(4,1)} %bitcast.7), calls=%async_computation.7 | async-start | bytes 8388608
  12.9 7.4 %collective-permute-start.5 = (f32[17,16,128]{2,1,0:T(8,128)S(1)}, f32[17,16,128]{2,1,0:T(8,128)S(1)}, u32[]{:S(2)}, u32[]{:S(2)}) collective-permute-start(f32[17,16,128]{2,1,0:T(8,128)S(1)} %add_add_fusion.q0), channel_id=1, source_target_pairs={{0,96},{32,64},{64,32},{96,0},{1,97},{33,65},{65,33},{97,1},{2,98}... | collective-permute-start | bytes 417800 | tf_op jit(solution)/shard_map/ppermute | solution.py:42
  16.9 5.5 %collective-permute-start.4 = (f32[17,16,128]{2,1,0:T(8,128)S(1)}, f32[17,16,128]{2,1,0:T(8,128)S(1)}, u32[]{:S(2)}, u32[]{:S(2)}) collective-permute-start(f32[17,16,128]{2,1,0:T(8,128)S(1)} %add_add_fusion.q0), channel_id=1, source_target_pairs={{0,64},{32,96},{64,0},{96,32},{1,65},{33,97},{65,1},{97,33},{2,66}... | collective-permute-start | bytes 417800 | tf_op jit(solution)/shard_map/ppermute | solution.py:42
  16.9 5.5 %collective-permute-start.3 = (f32[17,16,128]{2,1,0:T(8,128)S(1)}, f32[17,16,128]{2,1,0:T(8,128)S(1)}, u32[]{:S(2)}, u32[]{:S(2)}) collective-permute-start(f32[17,16,128]{2,1,0:T(8,128)S(1)} %add_add_fusion.q0), channel_id=1, source_target_pairs={{0,32},{32,0},{64,96},{96,64},{1,33},{33,1},{65,97},{97,65},{2,34}... | collective-permute-start | bytes 417800 | tf_op jit(solution)/shard_map/ppermute | solution.py:42
  22.4 24.5 %copy-start.9 = (f32[16]{0:T(128)S(1)}, f32[16]{0:T(128)}, u32[]{:S(2)}) copy-start(f32[16]{0:T(128)} %param.20) | copy-start | bytes 196
  22.4 24.6 %copy-start = (bf16[2048,256]{1,0:T(8,128)(2,1)S(1)}, bf16[2048,256]{1,0:T(8,128)(2,1)}, u32[]{:S(2)}) copy-start(bf16[2048,256]{1,0:T(8,128)(2,1)} %w_ref.5) | copy-start | bytes 3145732
  22.5 24.6 %copy-start.4 = (bf16[16,256]{1,0:T(8,128)(2,1)S(1)}, bf16[16,256]{1,0:T(8,128)(2,1)}, u32[]{:S(2)}) copy-start(bf16[16,256]{1,0:T(8,128)(2,1)} %tok_ref.1) | copy-start | bytes 24580
  22.5 24.6 %copy-start.6 = (f32[128]{0:T(128)S(1)}, f32[128]{0:T(128)}, u32[]{:S(2)}) copy-start(f32[128]{0:T(128)} %param.21) | copy-start | bytes 1540
  22.5 40.1 %copy-start.2 = (bf16[256,2048]{1,0:T(8,128)(2,1)S(1)}, bf16[256,2048]{1,0:T(8,128)(2,1)}, u32[]{:S(2)}) copy-start(bf16[256,2048]{1,0:T(8,128)(2,1)} %w_ref.6) | copy-start | bytes 3145732
  22.5 40.1 %copy-start.5 = (f32[256]{0:T(256)S(1)}, f32[256]{0:T(256)}, u32[]{:S(2)}) copy-start(f32[256]{0:T(256)} %param.23) | copy-start | bytes 3076
  22.5 70.1 %copy-start.3 = (bf16[2048,256]{1,0:T(8,128)(2,1)S(1)}, bf16[2048,256]{1,0:T(8,128)(2,1)}, u32[]{:S(2)}) copy-start(bf16[2048,256]{1,0:T(8,128)(2,1)} %w_ref.7) | copy-start | bytes 3145732
  27.6 7.0 %collective-permute-start.8 = (bf16[608,128]{1,0:T(8,128)(2,1)S(1)}, bf16[608,128]{1,0:T(8,128)(2,1)S(1)}, u32[]{:S(2)}, u32[]{:S(2)}) collective-permute-start(bf16[608,128]{1,0:T(8,128)(2,1)S(1)} %get-tuple-element.9.p0), channel_id=1, source_target_pairs={{0,24},{8,16},{16,8},{24,0},{1,25},{9,17},{17,9},{25,1},{2,26},{10... | collective-permute-start | bytes 466952 | tf_op jit(solution)/shard_map/ppermute | solution.py:42
  30.7 5.7 %collective-permute-start.7 = (bf16[608,128]{1,0:T(8,128)(2,1)S(1)}, bf16[608,128]{1,0:T(8,128)(2,1)S(1)}, u32[]{:S(2)}, u32[]{:S(2)}) collective-permute-start(bf16[608,128]{1,0:T(8,128)(2,1)S(1)} %get-tuple-element.9.p0), channel_id=1, source_target_pairs={{0,16},{8,24},{16,0},{24,8},{1,17},{9,25},{17,1},{25,9},{2,18},{10... | collective-permute-start | bytes 466952 | tf_op jit(solution)/shard_map/ppermute | solution.py:42
  30.9 5.5 %collective-permute-start.6 = (bf16[608,128]{1,0:T(8,128)(2,1)S(1)}, bf16[608,128]{1,0:T(8,128)(2,1)S(1)}, u32[]{:S(2)}, u32[]{:S(2)}) collective-permute-start(bf16[608,128]{1,0:T(8,128)(2,1)S(1)} %get-tuple-element.9.p0), channel_id=1, source_target_pairs={{0,8},{8,0},{16,24},{24,16},{1,9},{9,1},{17,25},{25,17},{2,10},{10... | collective-permute-start | bytes 466952 | tf_op jit(solution)/shard_map/ppermute | solution.py:42
  36.9 8.2 %collective-permute-start.11 = (bf16[608,128]{1,0:T(8,128)(2,1)S(1)}, bf16[608,128]{1,0:T(8,128)(2,1)S(1)}, u32[]{:S(2)}, u32[]{:S(2)}) collective-permute-start(bf16[608,128]{1,0:T(8,128)(2,1)S(1)} %merge.1.p0), channel_id=1, source_target_pairs={{0,96},{32,64},{64,32},{96,0},{1,97},{33,65},{65,33},{97,1},{2,98}... | collective-permute-start | bytes 466952 | tf_op jit(solution)/shard_map/ppermute | solution.py:42
  41.3 5.7 %collective-permute-start.10 = (bf16[608,128]{1,0:T(8,128)(2,1)S(1)}, bf16[608,128]{1,0:T(8,128)(2,1)S(1)}, u32[]{:S(2)}, u32[]{:S(2)}) collective-permute-start(bf16[608,128]{1,0:T(8,128)(2,1)S(1)} %merge.1.p0), channel_id=1, source_target_pairs={{0,64},{32,96},{64,0},{96,32},{1,65},{33,97},{65,1},{97,33},{2,66}... | collective-permute-start | bytes 466952 | tf_op jit(solution)/shard_map/ppermute | solution.py:42
  41.3 5.7 %collective-permute-start.9 = (bf16[608,128]{1,0:T(8,128)(2,1)S(1)}, bf16[608,128]{1,0:T(8,128)(2,1)S(1)}, u32[]{:S(2)}, u32[]{:S(2)}) collective-permute-start(bf16[608,128]{1,0:T(8,128)(2,1)S(1)} %merge.1.p0), channel_id=1, source_target_pairs={{0,32},{32,0},{64,96},{96,64},{1,33},{33,1},{65,97},{97,65},{2,34}... | collective-permute-start | bytes 466952 | tf_op jit(solution)/shard_map/ppermute | solution.py:42
  (2 other events, 2.0 us)

commit v3 on v2

--- a/solution.py
+++ b/solution.py
@@ -180,8 +180,8 @@
 
 
 def residual_body(
-    rows, vecs, ctx, p0, p1, p2, p3, inv_ref, lam_ref, gain_ref, tok_ref, w_ref,
-    res_ref, all_ref, nk_ref, nv_ref, n_scr,
+    rows, vecs, ctx, p0, p1, p2, p3, lam_ref, gain_ref, tok_ref, w_ref,
+    res_ref, all_ref, kv_ref, n_scr,
 ):
     refs = (p0, p1, p2, p3)
     heads = vecs // 2
@@ -208,11 +208,7 @@
         all_ref[t] = res
     rest = at + vecs
     a, b_, c, d = [r[rest:].astype(F32) for r in refs]
-    kv = (a + b_) + (c + d)
-    inv = inv_ref[...]
-    for t in range(2):
-        nk_ref[:, t, :] = (kv[t * rows : (t + 1) * rows] * inv).astype(BF16)
-        nv_ref[:, t, :] = (kv[(2 + t) * rows : (3 + t) * rows] * inv).astype(BF16)
+    kv_ref[...] = (a + b_) + (c + d)
 
 
 def diagonal(size):
@@ -259,11 +255,16 @@
     out_ref[...] = down.reshape(out_ref.shape)
 
 
-def final_body(down_ref, res_ref, out_ref):
+def final_body(down_ref, res_ref, kv_ref, inv_ref, out_ref, nk_ref, nv_ref):
     total = down_ref[0].astype(F32)
     for t in range(1, down_ref.shape[0]):
         total = total + down_ref[t].astype(F32)
     out_ref[...] = (res_ref[...].astype(F32) + total).astype(BF16)
+    rows = inv_ref.shape[0]
+    inv = inv_ref[...]
+    for t in range(2):
+        nk_ref[:, t, :] = (kv_ref[t * rows : (t + 1) * rows] * inv).astype(BF16)
+        nv_ref[:, t, :] = (kv_ref[(2 + t) * rows : (3 + t) * rows] * inv).astype(BF16)
 
 
 def shards(
@@ -344,18 +345,16 @@
         *from_peers(payload, "x"),
         flops=packed * LANES * 8,
     )
-    residual, to_all, new_keys, new_values = local_call(
+    residual, to_all, kv_sum = local_call(
         functools.partial(residual_body, rows, vecs, float(ctx)),
         "residual",
         (
             struct((rows, tok_width), BF16),
             struct((n_tp, rows, tok_width), BF16),
-            struct((rows, kv_heads, LANES), BF16),
-            struct((rows, kv_heads, LANES), BF16),
+            struct((4 * rows, LANES), F32),
         ),
         payload,
         *from_peers(payload, "z"),
-        inv_one,
         jnp.broadcast_to(lambdas[:, None], (heads, LANES)),
         head_gain[None, :],
         tokens,
@@ -388,12 +387,18 @@
         w_down,
         flops=2 * batch * tok_width * n_kv * LANES,
     )
-    mixed = local_call(
+    mixed, new_keys, new_values = local_call(
         final_body,
         "final",
-        struct((rows, tok_width), BF16),
+        (
+            struct((rows, tok_width), BF16),
+            struct((rows, kv_heads, LANES), BF16),
+            struct((rows, kv_heads, LANES), BF16),
+        ),
         exchanged(down, TP),
         residual,
+        kv_sum,
+        inv_one,
         flops=rows * tok_width * 10,
     )
     return mixed, new_keys, new_values

time: 104 us -> 104 us (level)
  no operation moved by 1% of the time
where the time goes in v3:
time: 104 us; the launch traced here: 103 us
  blocking collectives  53.4 us (51%)
  waiting for transfers between devices  18.6 us (18%)
  starting transfers between devices  17.5 us (17%)
  Pallas kernels  8.81 us (8%)
  local copies, waits for them, and re-layouts  3.4 us (3%)
    all_to_all x4, blocking collectives, exchanged(): return lax.all_to_all(tiles, axis, 0, 0, tiled=True)  53.4 us
    ppermute x12, waiting for transfers between devices, from_peers(): lax.ppermute(shard, axis, [(i, i ^ k) for i in range(peers)])  18.6 us
    ppermute x12, starting transfers between devices, from_peers(): lax.ppermute(shard, axis, [(i, i ^ k) for i in range(peers)])  17.5 us
    pallas_call x9, Pallas kernels, local_call(): pl.pallas_call(body, name=name, out_shape=outs, in_specs=[HBM if i in far...  8.81 us
    unnamed x28, local copies, waits for them, and re-layouts  3.26 us
  transfers between devices with their start and end apart: 12, of which 8 were waited for; matrix products, arithmetic and copies ran while one was open for 0% of the time, Pallas kernels for 0%

profile of v3, /device:TPU:1, one launch (start us, length us, event | category | flops | bytes accessed | tf_op | source)
XLA Modules:
  0.0 103.3 jit_solution(14319811892561939969)
XLA Ops:
  0.6 0.8 fusion.1
  1.5 1.2 %copy-done.1 = bf16[256,2048]{1,0:T(8,128)(2,1)S(1)} copy-done((bf16[256,2048]{1,0:T(8,128)(2,1)S(1)}, bf16[256,2048]{1,0:T(8,128)(2,1)}, u32[]{:S(2)}) %copy-start.1) | copy-done | bytes 1048600
  3.0 3.3 %collective-permute-start.2 = (f32[17,16,128]{2,1,0:T(8,128)S(1)}, f32[17,16,128]{2,1,0:T(8,128)S(1)}, u32[]{:S(2)}, u32[]{:S(2)}) collective-permute-start(f32[17,16,128]{2,1,0:T(8,128)S(1)} %query.1), channel_id=1, source_target_pairs={{0,24},{8,16},{16,8},{24,0},{1,25},{9,17},{17,9},{25,1},{2,26},{10... | collective-permute-start | bytes 417800 | tf_op jit(solution)/shard_map/ppermute | solution.py:42
  7.0 5.2 %collective-permute-done.2 = f32[17,16,128]{2,1,0:T(8,128)S(1)} collective-permute-done((f32[17,16,128]{2,1,0:T(8,128)S(1)}, f32[17,16,128]{2,1,0:T(8,128)S(1)}, u32[]{:S(2)}, u32[]{:S(2)}) %collective-permute-start.2) | collective-permute-done | bytes 139296 | tf_op jit(solution)/shard_map/ppermute | solution.py:42
  12.2 0.7 collective-permute-done
  12.9 3.9 %collective-permute-start.5 = (f32[17,16,128]{2,1,0:T(8,128)S(1)}, f32[17,16,128]{2,1,0:T(8,128)S(1)}, u32[]{:S(2)}, u32[]{:S(2)}) collective-permute-start(f32[17,16,128]{2,1,0:T(8,128)S(1)} %add_add_fusion.q0), channel_id=1, source_target_pairs={{0,96},{32,64},{64,32},{96,0},{1,97},{33,65},{65,33},{97,1},{2,98}... | collective-permute-start | bytes 417800 | tf_op jit(solution)/shard_map/ppermute | solution.py:42
  16.9 0.7 collective-permute-start.3
  17.5 1.1 %copy-done.7 = bf16[256,256]{1,0:T(8,128)(2,1)S(1)} copy-done((bf16[256,256]{1,0:T(8,128)(2,1)S(1)}, bf16[256,256]{1,0:T(8,128)(2,1)}, u32[]{:S(2)}) %copy-start.7) | copy-done | bytes 131096
  18.6 0.9 copy-done.8
  19.6 0.7 collective-permute-done.5.q3
  20.4 2.0 %collective-permute-done.4.q2 = f32[17,16,128]{2,1,0:T(8,128)S(1)} collective-permute-done((f32[17,16,128]{2,1,0:T(8,128)S(1)}, f32[17,16,128]{2,1,0:T(8,128)S(1)}, u32[]{:S(2)}, u32[]{:S(2)}) %collective-permute-start.4) | collective-permute-done | bytes 139296 | tf_op jit(solution)/shard_map/ppermute | solution.py:42
  22.5 5.1 %attention.1 = (bf16[608,128]{1,0:T(8,128)(2,1)S(1)}, f32[16,128]{1,0:T(8,128)S(1)}) custom-call(f32[17,16,128]{2,1,0:T(8,128)S(1)} %add_add_fusion.q0, f32[17,16,128]{2,1,0:T(8,128)S(1)} %collective-permute-done.3.q1, f32[17,16,128]{2,1,0:T(8,128)S(1)} %collective-permute-done.4.q2, f32[17,16,128]{2,1,0:T(8,128)S(1)} %collective-permute-done.5.q3, ...), custom_call_target="tpu_custom_call" | custom-call | flops 536870912 | bytes 17350656 | tf_op jit(solution)/shard_map/attention/pallas_call | solution.py:27
  27.6 3.1 %collective-permute-start.8 = (bf16[608,128]{1,0:T(8,128)(2,1)S(1)}, bf16[608,128]{1,0:T(8,128)(2,1)S(1)}, u32[]{:S(2)}, u32[]{:S(2)}) collective-permute-start(bf16[608,128]{1,0:T(8,128)(2,1)S(1)} %get-tuple-element.8.p0), channel_id=1, source_target_pairs={{0,24},{8,16},{16,8},{24,0},{1,25},{9,17},{17,9},{25,1},{2,26},{10... | collective-permute-start | bytes 466952 | tf_op jit(solution)/shard_map/ppermute | solution.py:42
  31.4 3.2 %collective-permute-done.8.p3 = bf16[608,128]{1,0:T(8,128)(2,1)S(1)} collective-permute-done((bf16[608,128]{1,0:T(8,128)(2,1)S(1)}, bf16[608,128]{1,0:T(8,128)(2,1)S(1)}, u32[]{:S(2)}, u32[]{:S(2)}) %collective-permute-start.8) | collective-permute-done | bytes 155680 | tf_op jit(solution)/shard_map/ppermute | solution.py:42
  34.6 1.8 %collective-permute-done.7.p2 = bf16[608,128]{1,0:T(8,128)(2,1)S(1)} collective-permute-done((bf16[608,128]{1,0:T(8,128)(2,1)S(1)}, bf16[608,128]{1,0:T(8,128)(2,1)S(1)}, u32[]{:S(2)}, u32[]{:S(2)}) %collective-permute-start.7) | collective-permute-done | bytes 155680 | tf_op jit(solution)/shard_map/ppermute | solution.py:42
  36.9 4.4 %collective-permute-start.11 = (bf16[608,128]{1,0:T(8,128)(2,1)S(1)}, bf16[608,128]{1,0:T(8,128)(2,1)S(1)}, u32[]{:S(2)}, u32[]{:S(2)}) collective-permute-start(bf16[608,128]{1,0:T(8,128)(2,1)S(1)} %merge.1.p0), channel_id=1, source_target_pairs={{0,96},{32,64},{64,32},{96,0},{1,97},{33,65},{65,33},{97,1},{2,98}... | collective-permute-start | bytes 466952 | tf_op jit(solution)/shard_map/ppermute | solution.py:42
  41.3 0.7 collective-permute-start.9
  41.9 3.2 %collective-permute-done.11.p3 = bf16[608,128]{1,0:T(8,128)(2,1)S(1)} collective-permute-done((bf16[608,128]{1,0:T(8,128)(2,1)S(1)}, bf16[608,128]{1,0:T(8,128)(2,1)S(1)}, u32[]{:S(2)}, u32[]{:S(2)}) %collective-permute-start.11) | collective-permute-done | bytes 155680 | tf_op jit(solution)/shard_map/ppermute | solution.py:42
  45.1 1.8 %collective-permute-done.10.p2 = bf16[608,128]{1,0:T(8,128)(2,1)S(1)} collective-permute-done((bf16[608,128]{1,0:T(8,128)(2,1)S(1)}, bf16[608,128]{1,0:T(8,128)(2,1)S(1)}, u32[]{:S(2)}, u32[]{:S(2)}) %collective-permute-start.10) | collective-permute-done | bytes 155680 | tf_op jit(solution)/shard_map/ppermute | solution.py:42
  47.1 1.5 %residual.1 = (bf16[16,256]{1,0:T(8,128)(2,1)S(1)}, bf16[8,16,256]{2,1,0:T(8,128)(2,1)S(1)}, f32[64,128]{1,0:T(8,128)S(1)}) custom-call(bf16[608,128]{1,0:T(8,128)(2,1)S(1)} %merge.1.p0, bf16[608,128]{1,0:T(8,128)(2,1)S(1)} %collective-permute-done.9.p1, bf16[608,128]{1,0:T(8,128)(2,1)S(1)} %collective-permute-done.10.p2, ...), custom_call_target="tpu_custom_call" | custom-call | flops 16777216 | bytes 1688064 | tf_op jit(solution)/shard_map/residual/pallas_call | solution.py:27
  48.5 13.5 %all_to_all.20.res_ref = bf16[8,16,256]{2,1,0:T(8,128)(2,1)S(1)} all-to-all(bf16[8,16,256]{2,1,0:T(8,128)(2,1)S(1)} %get-tuple-element.9), channel_id=1, replica_groups=mesh['z'=4,'x'=4,'y'=4,'c'=2] {'y','c'}, dimensions={0} | all-to-all | bytes 131072 | tf_op jit(solution)/shard_map/all_to_all | solution.py:48
  62.4 17.2 %all_to_all.21.in_ref = bf16[16,144,128]{2,1,0:T(8,128)(2,1)S(1)} all-to-all(bf16[16,144,128]{2,1,0:T(8,128)(2,1)S(1)} %up.1), channel_id=1, replica_groups=mesh['z'=4,'x'=4,'y'=4,'c'=2] {'z','x'}, dimensions={0} | all-to-all | bytes 1179648 | tf_op jit(solution)/shard_map/all_to_all | solution.py:48
  79.7 12.3 %all_to_all.22.act_ref = bf16[16,128,128]{2,1,0:T(8,128)(2,1)S(1)} all-to-all(bf16[16,128,128]{2,1,0:T(8,128)(2,1)S(1)} %act.1), channel_id=1, replica_groups=mesh['z'=4,'x'=4,'y'=4,'c'=2] {'z','x'}, dimensions={0} | all-to-all | bytes 1048576 | tf_op jit(solution)/shard_map/all_to_all | solution.py:48
  92.4 10.3 %all_to_all.23.down_ref = bf16[8,16,256]{2,1,0:T(8,128)(2,1)S(1)} all-to-all(bf16[8,16,256]{2,1,0:T(8,128)(2,1)S(1)} %down.1), channel_id=1, replica_groups=mesh['z'=4,'x'=4,'y'=4,'c'=2] {'y','c'}, dimensions={0} | all-to-all | bytes 131072 | tf_op jit(solution)/shard_map/all_to_all | solution.py:48
  (47 shorter events, 3.9 us)
Async XLA Ops:
  1.5 1.2 %copy-start.1 = (bf16[256,2048]{1,0:T(8,128)(2,1)S(1)}, bf16[256,2048]{1,0:T(8,128)(2,1)}, u32[]{:S(2)}) copy-start(bf16[256,2048]{1,0:T(8,128)(2,1)} %w_ref.4) | copy-start | bytes 3145732
  3.0 9.2 %collective-permute-start.2 = (f32[17,16,128]{2,1,0:T(8,128)S(1)}, f32[17,16,128]{2,1,0:T(8,128)S(1)}, u32[]{:S(2)}, u32[]{:S(2)}) collective-permute-start(f32[17,16,128]{2,1,0:T(8,128)S(1)} %query.1), channel_id=1, source_target_pairs={{0,24},{8,16},{16,8},{24,0},{1,25},{9,17},{17,9},{25,1},{2,26},{10... | collective-permute-start | bytes 417800 | tf_op jit(solution)/shard_map/ppermute | solution.py:42
  6.3 5.9 %collective-permute-start.1 = (f32[17,16,128]{2,1,0:T(8,128)S(1)}, f32[17,16,128]{2,1,0:T(8,128)S(1)}, u32[]{:S(2)}, u32[]{:S(2)}) collective-permute-start(f32[17,16,128]{2,1,0:T(8,128)S(1)} %query.1), channel_id=1, source_target_pairs={{0,16},{8,24},{16,0},{24,8},{1,17},{9,25},{17,1},{25,9},{2,18},{10... | collective-permute-start | bytes 417800 | tf_op jit(solution)/shard_map/ppermute | solution.py:42
  6.8 6.0 %collective-permute-start = (f32[17,16,128]{2,1,0:T(8,128)S(1)}, f32[17,16,128]{2,1,0:T(8,128)S(1)}, u32[]{:S(2)}, u32[]{:S(2)}) collective-permute-start(f32[17,16,128]{2,1,0:T(8,128)S(1)} %query.1), channel_id=1, source_target_pairs={{0,8},{8,0},{16,24},{24,16},{1,9},{9,1},{17,25},{25,17},{2,10},{10... | collective-permute-start | bytes 417800 | tf_op jit(solution)/shard_map/ppermute | solution.py:42
  12.8 9.5 %slice-start = ((s8[8388608]{0:T(1024)(128)(4,1)}), s8[4194304]{0:T(1024)(128)(4,1)S(1)}, s32[]{:S(2)}) async-start(s8[8388608]{0:T(1024)(128)(4,1)} %bitcast.4), calls=%async_computation.4 | async-start | bytes 8388608
  12.9 9.5 %slice-start.2 = ((s8[8388608]{0:T(1024)(128)(4,1)}), s8[4194304]{0:T(1024)(128)(4,1)S(1)}, s32[]{:S(2)}) async-start(s8[8388608]{0:T(1024)(128)(4,1)} %bitcast.7), calls=%async_computation.6 | async-start | bytes 8388608
  12.9 9.5 %slice-start.1 = ((s8[8388608]{0:T(1024)(128)(4,1)}), s8[4194304]{0:T(1024)(128)(4,1)S(1)}, s32[]{:S(2)}) async-start(s8[8388608]{0:T(1024)(128)(4,1)} %bitcast.4), calls=%async_computation.5 | async-start | bytes 8388608
  12.9 9.5 %slice-start.3 = ((s8[8388608]{0:T(1024)(128)(4,1)}), s8[4194304]{0:T(1024)(128)(4,1)S(1)}, s32[]{:S(2)}) async-start(s8[8388608]{0:T(1024)(128)(4,1)} %bitcast.7), calls=%async_computation.7 | async-start | bytes 8388608
  12.9 7.4 %collective-permute-start.5 = (f32[17,16,128]{2,1,0:T(8,128)S(1)}, f32[17,16,128]{2,1,0:T(8,128)S(1)}, u32[]{:S(2)}, u32[]{:S(2)}) collective-permute-start(f32[17,16,128]{2,1,0:T(8,128)S(1)} %add_add_fusion.q0), channel_id=1, source_target_pairs={{0,96},{32,64},{64,32},{96,0},{1,97},{33,65},{65,33},{97,1},{2,98}... | collective-permute-start | bytes 417800 | tf_op jit(solution)/shard_map/ppermute | solution.py:42
  16.9 5.5 %collective-permute-start.4 = (f32[17,16,128]{2,1,0:T(8,128)S(1)}, f32[17,16,128]{2,1,0:T(8,128)S(1)}, u32[]{:S(2)}, u32[]{:S(2)}) collective-permute-start(f32[17,16,128]{2,1,0:T(8,128)S(1)} %add_add_fusion.q0), channel_id=1, source_target_pairs={{0,64},{32,96},{64,0},{96,32},{1,65},{33,97},{65,1},{97,33},{2,66}... | collective-permute-start | bytes 417800 | tf_op jit(solution)/shard_map/ppermute | solution.py:42
  16.9 5.5 %collective-permute-start.3 = (f32[17,16,128]{2,1,0:T(8,128)S(1)}, f32[17,16,128]{2,1,0:T(8,128)S(1)}, u32[]{:S(2)}, u32[]{:S(2)}) collective-permute-start(f32[17,16,128]{2,1,0:T(8,128)S(1)} %add_add_fusion.q0), channel_id=1, source_target_pairs={{0,32},{32,0},{64,96},{96,64},{1,33},{33,1},{65,97},{97,65},{2,34}... | collective-permute-start | bytes 417800 | tf_op jit(solution)/shard_map/ppermute | solution.py:42
  22.4 24.5 %copy-start.9 = (f32[16]{0:T(128)S(1)}, f32[16]{0:T(128)}, u32[]{:S(2)}) copy-start(f32[16]{0:T(128)} %param.20) | copy-start | bytes 196
  22.4 24.6 %copy-start = (bf16[2048,256]{1,0:T(8,128)(2,1)S(1)}, bf16[2048,256]{1,0:T(8,128)(2,1)}, u32[]{:S(2)}) copy-start(bf16[2048,256]{1,0:T(8,128)(2,1)} %w_ref.5) | copy-start | bytes 3145732
  22.5 24.6 %copy-start.4 = (bf16[16,256]{1,0:T(8,128)(2,1)S(1)}, bf16[16,256]{1,0:T(8,128)(2,1)}, u32[]{:S(2)}) copy-start(bf16[16,256]{1,0:T(8,128)(2,1)} %tok_ref.1) | copy-start | bytes 24580
  22.5 24.6 %copy-start.6 = (f32[128]{0:T(128)S(1)}, f32[128]{0:T(128)}, u32[]{:S(2)}) copy-start(f32[128]{0:T(128)} %param.21) | copy-start | bytes 1540
  22.5 39.6 %copy-start.2 = (bf16[256,2048]{1,0:T(8,128)(2,1)S(1)}, bf16[256,2048]{1,0:T(8,128)(2,1)}, u32[]{:S(2)}) copy-start(bf16[256,2048]{1,0:T(8,128)(2,1)} %w_ref.6) | copy-start | bytes 3145732
  22.5 39.6 %copy-start.5 = (f32[256]{0:T(256)S(1)}, f32[256]{0:T(256)}, u32[]{:S(2)}) copy-start(f32[256]{0:T(256)} %param.23) | copy-start | bytes 3076
  22.5 69.6 %copy-start.3 = (bf16[2048,256]{1,0:T(8,128)(2,1)S(1)}, bf16[2048,256]{1,0:T(8,128)(2,1)}, u32[]{:S(2)}) copy-start(bf16[2048,256]{1,0:T(8,128)(2,1)} %w_ref.7) | copy-start | bytes 3145732
  27.6 7.0 %collective-permute-start.8 = (bf16[608,128]{1,0:T(8,128)(2,1)S(1)}, bf16[608,128]{1,0:T(8,128)(2,1)S(1)}, u32[]{:S(2)}, u32[]{:S(2)}) collective-permute-start(bf16[608,128]{1,0:T(8,128)(2,1)S(1)} %get-tuple-element.8.p0), channel_id=1, source_target_pairs={{0,24},{8,16},{16,8},{24,0},{1,25},{9,17},{17,9},{25,1},{2,26},{10... | collective-permute-start | bytes 466952 | tf_op jit(solution)/shard_map/ppermute | solution.py:42
  30.7 5.7 %collective-permute-start.7 = (bf16[608,128]{1,0:T(8,128)(2,1)S(1)}, bf16[608,128]{1,0:T(8,128)(2,1)S(1)}, u32[]{:S(2)}, u32[]{:S(2)}) collective-permute-start(bf16[608,128]{1,0:T(8,128)(2,1)S(1)} %get-tuple-element.8.p0), channel_id=1, source_target_pairs={{0,16},{8,24},{16,0},{24,8},{1,17},{9,25},{17,1},{25,9},{2,18},{10... | collective-permute-start | bytes 466952 | tf_op jit(solution)/shard_map/ppermute | solution.py:42
  30.9 5.5 %collective-permute-start.6 = (bf16[608,128]{1,0:T(8,128)(2,1)S(1)}, bf16[608,128]{1,0:T(8,128)(2,1)S(1)}, u32[]{:S(2)}, u32[]{:S(2)}) collective-permute-start(bf16[608,128]{1,0:T(8,128)(2,1)S(1)} %get-tuple-element.8.p0), channel_id=1, source_target_pairs={{0,8},{8,0},{16,24},{24,16},{1,9},{9,1},{17,25},{25,17},{2,10},{10... | collective-permute-start | bytes 466952 | tf_op jit(solution)/shard_map/ppermute | solution.py:42
  36.9 8.2 %collective-permute-start.11 = (bf16[608,128]{1,0:T(8,128)(2,1)S(1)}, bf16[608,128]{1,0:T(8,128)(2,1)S(1)}, u32[]{:S(2)}, u32[]{:S(2)}) collective-permute-start(bf16[608,128]{1,0:T(8,128)(2,1)S(1)} %merge.1.p0), channel_id=1, source_target_pairs={{0,96},{32,64},{64,32},{96,0},{1,97},{33,65},{65,33},{97,1},{2,98}... | collective-permute-start | bytes 466952 | tf_op jit(solution)/shard_map/ppermute | solution.py:42
  41.3 5.7 %collective-permute-start.10 = (bf16[608,128]{1,0:T(8,128)(2,1)S(1)}, bf16[608,128]{1,0:T(8,128)(2,1)S(1)}, u32[]{:S(2)}, u32[]{:S(2)}) collective-permute-start(bf16[608,128]{1,0:T(8,128)(2,1)S(1)} %merge.1.p0), channel_id=1, source_target_pairs={{0,64},{32,96},{64,0},{96,32},{1,65},{33,97},{65,1},{97,33},{2,66}... | collective-permute-start | bytes 466952 | tf_op jit(solution)/shard_map/ppermute | solution.py:42
  41.3 5.7 %collective-permute-start.9 = (bf16[608,128]{1,0:T(8,128)(2,1)S(1)}, bf16[608,128]{1,0:T(8,128)(2,1)S(1)}, u32[]{:S(2)}, u32[]{:S(2)}) collective-permute-start(bf16[608,128]{1,0:T(8,128)(2,1)S(1)} %merge.1.p0), channel_id=1, source_target_pairs={{0,32},{32,0},{64,96},{96,64},{1,33},{33,1},{65,97},{97,65},{2,34}... | collective-permute-start | bytes 466952 | tf_op jit(solution)/shard_map/ppermute | solution.py:42
  (2 other events, 2.0 us)

commit v4 on v3

--- a/solution.py
+++ b/solution.py
@@ -11,6 +11,7 @@
 KV = ("z", "x")
 TP = ("y", "c")
 EPS = 1e-06
+TAIL = 8
 LANES = 128
 F32 = jnp.float32
 BF16 = jnp.bfloat16
@@ -59,32 +60,25 @@
     return hi, mid, lo
 
 
-def query_body(scaled_ref, squares_ref, w_ref, q_ref):
-    q = dot(scaled_ref[...], w_ref[...])
-    tiles = q_ref.shape[0] - 1
-    for h in range(tiles):
-        q_ref[h] = q[:, h * LANES : (h + 1) * LANES]
-    q_ref[tiles] = squares_ref[...]
-
-
 def new_kv_body(scaled_ref, wk_ref, wv_ref, kv_ref):
-    rows = scaled_ref.shape[0]
     at = 0
     for w in (wk_ref, wv_ref):
-        part = dot(scaled_ref[...], w[...]).astype(BF16)
+        part = dot(scaled_ref[...], w[...])
         for t in range(part.shape[1] // LANES):
-            kv_ref[at : at + rows] = part[:, t * LANES : (t + 1) * LANES]
-            at += rows
-
-
-def attention_body(width, q0, q1, q2, q3, kv_ref, k_ref, v_ref, out_ref, inv_ref, q_scr, s_scr):
+            kv_ref[at] = part[:, t * LANES : (t + 1) * LANES]
+            at += 1
+
+
+def attention_body(width, q_ref, kv_ref, k_ref, v_ref, out_ref, q_scr, s_scr):
     rows, spots, _ = k_ref.shape
-    heads = q0.shape[0] - 1
-    total_q = (q0[...] + q1[...]) + (q2[...] + q3[...])
-    inv = lax.rsqrt(total_q[heads] / width + EPS)
-    inv_ref[...] = inv
+    heads = q_ref.shape[1] // LANES - 1
+    inv = lax.rsqrt(q_ref[:, heads * LANES :] * (32.0 / width) + EPS)
+    rest = rows * 2 * heads + 2 * heads
+    for t in range(kv_ref.shape[0]):
+        out_ref[rest + t * rows : rest + (t + 1) * rows] = (kv_ref[t] * inv).astype(BF16)
     for h in range(heads):
-        q_scr[:, h, :] = (total_q[h] * inv).astype(BF16).astype(F32) * 0.125
+        part = q_ref[:, h * LANES : (h + 1) * LANES] * 0.125 * inv
+        q_scr[h * rows : (h + 1) * rows] = part.astype(BF16).astype(F32) * 0.125
     vecs = 2 * heads
     lane = lax.broadcasted_iota(jnp.int32, (vecs, LANES), 1)
     row = lax.broadcasted_iota(jnp.int32, (vecs, LANES), 0)
@@ -94,7 +88,7 @@
     own_head = (wide_lane % 2) == ((wide_row % heads) // (heads // 2))
 
     def scores(b):
-        q16 = q_scr[b]
+        q16 = q_scr[pl.ds(b, heads, stride=rows), :]
         both = jnp.concatenate([q16, q16], axis=0)
         q32 = jnp.where(own_half, both, 0.0).astype(BF16)
         return dot(q32, k_ref[b], ((1,), (1,)))
@@ -111,7 +105,7 @@
             here & (lane < 48), top, jnp.where(here & (lane < 96), total, stats)
         )
 
-    deep = 4
+    deep = 16
     s_scr[0] = scores(0)
 
     def step(i, stats):
@@ -130,7 +124,6 @@
     out_ref[at : at + vecs] = jnp.where(
         kind == 0, hi, jnp.where(kind == 1, mid, lo)
     ).astype(BF16)
-    out_ref[at + vecs :] = kv_ref[...]
 
 
 def opened_stats(ref, at, vecs):
@@ -174,6 +167,7 @@
     out_ref[at : at + vecs] = jnp.where(
         kind == 0, hi, jnp.where(kind == 1, mid, lo)
     ).astype(BF16)
+
     rest = at + vecs
     a, b_, c, d = [r[rest:].astype(F32) for r in refs]
     out_ref[rest:] = ((a + b_) + (c + d)).astype(BF16)
@@ -181,7 +175,7 @@
 
 def residual_body(
     rows, vecs, ctx, p0, p1, p2, p3, lam_ref, gain_ref, tok_ref, w_ref,
-    res_ref, all_ref, kv_ref, n_scr,
+    res_ref, kv_ref, n_scr,
 ):
     refs = (p0, p1, p2, p3)
     heads = vecs // 2
@@ -200,12 +194,14 @@
         second = weighted(refs, weights, b, b * vecs + heads, heads, heads)
         out = first - second
         mean_sq = jnp.mean(out * out, axis=1, keepdims=True)
-        n_scr[:, b, :] = out * lax.rsqrt(mean_sq + 1.0 / ctx) * gain
-    normed = jnp.concatenate([n_scr[h].astype(BF16) for h in range(heads)], axis=1)
+        normed = out * lax.rsqrt(mean_sq + 1.0 / ctx) * gain
+        n_scr[b * heads : (b + 1) * heads] = normed
+    normed = jnp.concatenate(
+        [n_scr[pl.ds(h, rows, stride=heads), :].astype(BF16) for h in range(heads)],
+        axis=1,
+    )
     res = (tok_ref[...].astype(F32) + dot(normed, w_ref[...])).astype(BF16)
     res_ref[...] = res
-    for t in range(all_ref.shape[0]):
-        all_ref[t] = res
     rest = at + vecs
     a, b_, c, d = [r[rest:].astype(F32) for r in refs]
     kv_ref[...] = (a + b_) + (c + d)
@@ -216,15 +212,17 @@
     return a == lax.broadcasted_iota(jnp.int32, (size, size), 1)
 
 
-def up_body(res_ref, gain_ref, w_ref, out_ref):
-    groups, rows, width = res_ref.shape
-    batch = groups * rows
-    res = res_ref[...].reshape(batch, width).astype(F32)
+def up_body(r0, r1, r2, r3, gain_ref, w_ref, out_ref):
+    cores, rows, width = r0.shape
+    batch = 4 * cores * rows
+    res = jnp.concatenate(
+        [r[t].astype(F32) for r in (r0, r1, r2, r3) for t in range(cores)], axis=0
+    )
     gained = (res * gain_ref[...]).astype(BF16)
     squares = jnp.sum(res * res, axis=1, keepdims=True)
     line = jnp.sum(jnp.where(diagonal(batch), squares, 0.0), axis=0, keepdims=True)
-    hi, mid, lo = pieces(jnp.broadcast_to(line, (16, batch)))
-    sub = lax.broadcasted_iota(jnp.int32, (16, batch), 0)
+    hi, mid, lo = pieces(jnp.broadcast_to(line, (TAIL, batch)))
+    sub = lax.broadcasted_iota(jnp.int32, (TAIL, batch), 0)
     tail = jnp.where(sub == 0, hi, jnp.where(sub == 1, mid, jnp.where(sub == 2, lo, 0.0)))
     tail = tail.astype(BF16)
     up = dot(gained, w_ref[...])
@@ -248,23 +246,29 @@
         out_ref[p] = act
 
 
-def down_body(act_ref, w_ref, out_ref):
+def down_body(act_ref, w_ref, *out_refs):
     peers = act_ref.shape[0]
     acts = jnp.concatenate([act_ref[p] for p in range(peers)], axis=1)
     down = dot(acts, w_ref[...]).astype(BF16)
-    out_ref[...] = down.reshape(out_ref.shape)
-
-
-def final_body(down_ref, res_ref, kv_ref, inv_ref, out_ref, nk_ref, nv_ref):
-    total = down_ref[0].astype(F32)
-    for t in range(1, down_ref.shape[0]):
-        total = total + down_ref[t].astype(F32)
+    size = down.shape[0] // len(out_refs)
+    for k, out_ref in enumerate(out_refs):
+        out_ref[...] = down[k * size : (k + 1) * size].reshape(out_ref.shape)
+
+
+def sum_body(d0, d1, d2, d3, own_ref, other_ref):
+    a, b, c, d = [r[...].astype(F32) for r in (d0, d1, d2, d3)]
+    total = (a + b) + (c + d)
+    own_ref[...] = total[0]
+    other_ref[...] = total[1]
+
+
+def final_body(own_ref, other_ref, res_ref, kv_ref, out_ref, nk_ref, nv_ref):
+    total = own_ref[...] + other_ref[...]
     out_ref[...] = (res_ref[...].astype(F32) + total).astype(BF16)
-    rows = inv_ref.shape[0]
-    inv = inv_ref[...]
+    rows = out_ref.shape[0]
     for t in range(2):
-        nk_ref[:, t, :] = (kv_ref[t * rows : (t + 1) * rows] * inv).astype(BF16)
-        nv_ref[:, t, :] = (kv_ref[(2 + t) * rows : (3 + t) * rows] * inv).astype(BF16)
+        nk_ref[:, t, :] = kv_ref[t * rows : (t + 1) * rows].astype(BF16)
+        nv_ref[:, t, :] = kv_ref[(2 + t) * rows : (3 + t) * rows].astype(BF16)
 
 
 def shards(
@@ -297,43 +301,36 @@
     tok = tokens.astype(F32)
     scaled = (tok * attn_gain[None, :]).astype(BF16)
     squares = jnp.sum(tok * tok, axis=1, keepdims=True)
-    q_part = local_call(
-        query_body,
-        "query",
-        struct((heads + 1, rows, LANES), F32),
-        scaled,
-        jnp.broadcast_to(squares, (rows, LANES)),
-        w_query,
-        flops=2 * rows * tok_width * w_query.shape[1],
-    )
+    query = dot(scaled, w_query) * 32.0
+    spread = jnp.broadcast_to(squares * 0.125, (rows, LANES))
+    q_part = jnp.concatenate([query, spread], axis=1)
     kv_part = local_call(
         new_kv_body,
         "new_kv",
-        struct((4 * rows, LANES), BF16),
+        struct((4, rows, LANES), F32),
         scaled,
         w_key,
         w_value,
         flops=1 << 33,
     )
-    a, b, c = from_peers(q_part, "x")
-    q_half = (q_part + a) + (b + c)
-    a, b, c = from_peers(q_half, "z")
+    q_part = q_part.astype(jnp.float16)
+    a, b, c = [p.astype(F32) for p in from_peers(q_part, "z")]
+    q_half = (((q_part.astype(F32) + a) + (b + c)) * 0.25).astype(jnp.float16)
+    a, b, c = [p.astype(F32) for p in from_peers(q_half, "x")]
+    total_q = (q_half.astype(F32) + a) + (b + c)
     packed = rows * vecs + vecs + 4 * rows
-    payload, inv_one = local_call(
+    payload = local_call(
         functools.partial(attention_body, float(width)),
         "attention",
-        (struct((packed, LANES), BF16), struct((rows, LANES), F32)),
-        q_half,
-        a,
-        b,
-        c,
+        struct((packed, LANES), BF16),
+        total_q,
         kv_part,
         cache_keys.reshape(rows, spots, LANES),
         cache_values.reshape(rows, spots, LANES),
         flops=4 * rows * vecs * spots * LANES,
         limit=24,
         scratch=(
-            pltpu.VMEM((rows, heads, LANES), F32),
+            pltpu.VMEM((heads * rows, LANES), F32),
             pltpu.VMEM((2, vecs, spots), F32),
         ),
     )
@@ -345,12 +342,11 @@
         *from_peers(payload, "x"),
         flops=packed * LANES * 8,
     )
-    residual, to_all, kv_sum = local_call(
+    residual, kv_sum = local_call(
         functools.partial(residual_body, rows, vecs, float(ctx)),
         "residual",
         (
             struct((rows, tok_width), BF16),
-            struct((n_tp, rows, tok_width), BF16),
             struct((4 * rows, LANES), F32),
         ),
         payload,
@@ -360,14 +356,15 @@
         tokens,
         w_out,
         flops=2 * rows * heads * LANES * tok_width,
-        scratch=(pltpu.VMEM((heads, rows, LANES), F32),),
-    )
-    everyone = exchanged(to_all, TP)
+        scratch=(pltpu.VMEM((rows * heads, LANES), F32),),
+    )
+    pair = jnp.stack([residual, lax.ppermute(residual, "c", [(0, 1), (1, 0)])])
+    everyone = [pair, *from_peers(pair, "y")]
     up = local_call(
         up_body,
         "up",
-        struct((n_kv, batch + 16, LANES), BF16),
-        everyone,
+        struct((n_kv, batch + TAIL, LANES), BF16),
+        *everyone,
         mlp_gain[None, :],
         w_up,
         flops=2 * batch * tok_width * n_kv * LANES,
@@ -382,10 +379,23 @@
     down = local_call(
         down_body,
         "down",
-        struct((n_tp, rows, tok_width), BF16),
+        (struct((2, rows, tok_width), BF16),) * 4,
         exchanged(acts, KV),
         w_down,
         flops=2 * batch * tok_width * n_kv * LANES,
+    )
+    arrived = [
+        lax.ppermute(d, "y", [(i, i ^ k) for i in range(4)])
+        for k, d in enumerate(down)
+        if k
+    ]
+    own, other = local_call(
+        sum_body,
+        "sum",
+        (struct((rows, tok_width), F32),) * 2,
+        down[0],
+        *arrived,
+        flops=rows * tok_width * 16,
     )
     mixed, new_keys, new_values = local_call(
         final_body,
@@ -395,10 +405,10 @@
             struct((rows, kv_heads, LANES), BF16),
             struct((rows, kv_heads, LANES), BF16),
         ),
-        exchanged(down, TP),
+        own,
+        lax.ppermute(other, "c", [(0, 1), (1, 0)]),
         residual,
         kv_sum,
-        inv_one,
         flops=rows * tok_width * 10,
     )
     return mixed, new_keys, new_values

time: 104 us -> 95.5 us (0.918)
  blocking collectives: 53.4 us -> 25.9 us
  starting transfers between devices: 17.5 us -> 34.4 us
  waiting for transfers between devices: 18.6 us -> 21.5 us
    all_to_all x4 -> x2, blocking collectives: 53.4 us -> 25.9 us  [exchanged(): return lax.all_to_all(tiles, axis, 0, 0, tiled=True)]
    ppermute x0 -> x5, starting transfers between devices: none -> 15.9 us  [the longest x1 6.58 us: shards(): pair = jnp.stack([residual, lax.ppermute(residual, 'c', [(0, 1), (1, 0)])])]
    ppermute x0 -> x5, waiting for transfers between devices: none -> 3.84 us  [the longest x3 2.17 us: shards(): lax.ppermute(d, 'y', [(i, i ^ k) for i in range(4)])]
    ppermute x12 -> x15, starting transfers between devices: 17.5 us -> 18.5 us  [from_peers(): lax.ppermute(shard, axis, [(i, i ^ k) for i in range(peers)])]
    ppermute x12 -> x15, waiting for transfers between devices: 18.6 us -> 17.7 us  [from_peers(): lax.ppermute(shard, axis, [(i, i ^ k) for i in range(peers)])]
  transfers between devices with their start and end apart: 12 -> 20, of which waited for: 8 -> 16; matrix products, arithmetic and copies ran while one was open for 0% -> 0% of each run, Pallas kernels for 0% -> 0%
where the time goes in v4:
time: 95.5 us; the launch traced here: 95.3 us
  starting transfers between devices  34.4 us (36%)
  blocking collectives  25.9 us (27%)
  waiting for transfers between devices  21.5 us (23%)
  Pallas kernels  8.14 us (9%)
  local copies, waits for them, and re-layouts  3.15 us (3%)
  other arithmetic  1.03 us (1%)
    all_to_all x2, blocking collectives, exchanged(): return lax.all_to_all(tiles, axis, 0, 0, tiled=True)  25.9 us
    ppermute x15, starting transfers between devices, from_peers(): lax.ppermute(shard, axis, [(i, i ^ k) for i in range(peers)])  18.5 us
    ppermute x15, waiting for transfers between devices, from_peers(): lax.ppermute(shard, axis, [(i, i ^ k) for i in range(peers)])  17.7 us
    pallas_call x9, Pallas kernels, local_call(): pl.pallas_call(body, name=name, out_shape=outs, in_specs=[HBM if i in far...  8.14 us
    ppermute x1, starting transfers between devices, shards(): pair = jnp.stack([residual, lax.ppermute(residual, 'c', [(0, 1), (1, 0)])])  6.58 us
    ppermute x1, starting transfers between devices, shards(): lax.ppermute(other, 'c', [(0, 1), (1, 0)])  5.37 us
    ppermute x3, starting transfers between devices, shards(): lax.ppermute(d, 'y', [(i, i ^ k) for i in range(4)])  3.93 us
    unnamed x28, local copies, waits for them, and re-layouts  3 us
  transfers between devices with their start and end apart: 20, of which 16 were waited for; matrix products, arithmetic and copies ran while one was open for 0% of the time, Pallas kernels for 0%

profile of v4, /device:TPU:1, one launch (start us, length us, event | category | flops | bytes accessed | tf_op | source)
XLA Modules:
  0.0 95.3 jit_solution(487428225588293042)
XLA Ops:
  2.3 4.5 %collective-permute-start.1 = (f16[16,2176]{1,0:T(8,128)(2,1)S(1)}, f16[16,2176]{1,0:T(8,128)(2,1)S(1)}, u32[]{:S(2)}, u32[]{:S(2)}) collective-permute-start(f16[16,2176]{1,0:T(8,128)(2,1)S(1)} %pad_maximum_fusion), channel_id=1, source_target_pairs={{0,64},{32,96},{64,0},{96,32},{1,65},{33,97},{65,1},{97,33},{2,66}... | collective-permute-start | bytes 208904 | tf_op jit(solution)/shard_map/ppermute | solution.py:43
  8.4 1.8 %collective-permute-done = f16[16,2176]{1,0:T(8,128)(2,1)S(1)} collective-permute-done((f16[16,2176]{1,0:T(8,128)(2,1)S(1)}, f16[16,2176]{1,0:T(8,128)(2,1)S(1)}, u32[]{:S(2)}, u32[]{:S(2)}) %collective-permute-start) | collective-permute-done | bytes 69664 | tf_op jit(solution)/shard_map/ppermute | solution.py:43
  10.3 1.6 %collective-permute-done.2 = f16[16,2176]{1,0:T(8,128)(2,1)S(1)} collective-permute-done((f16[16,2176]{1,0:T(8,128)(2,1)S(1)}, f16[16,2176]{1,0:T(8,128)(2,1)S(1)}, u32[]{:S(2)}, u32[]{:S(2)}) %collective-permute-start.2) | collective-permute-done | bytes 69664 | tf_op jit(solution)/shard_map/ppermute | solution.py:43
  11.9 2.6 %collective-permute-start.5 = (f16[16,2176]{1,0:T(8,128)(2,1)S(1)}, f16[16,2176]{1,0:T(8,128)(2,1)S(1)}, u32[]{:S(2)}, u32[]{:S(2)}) collective-permute-start(f16[16,2176]{1,0:T(8,128)(2,1)S(1)} %multiply_convert_fusion), channel_id=1, source_target_pairs={{0,24},{8,16},{16,8},{24,0},{1,25},{9,17},{17,9},{25,1},{2,26},{10... | collective-permute-start | bytes 208904 | tf_op jit(solution)/shard_map/ppermute | solution.py:43
  15.3 1.7 %copy-done.7 = bf16[256,256]{1,0:T(8,128)(2,1)S(1)} copy-done((bf16[256,256]{1,0:T(8,128)(2,1)S(1)}, bf16[256,256]{1,0:T(8,128)(2,1)}, u32[]{:S(2)}) %copy-start.7) | copy-done | bytes 131096
  18.0 1.2 %collective-permute-done.4 = f16[16,2176]{1,0:T(8,128)(2,1)S(1)} collective-permute-done((f16[16,2176]{1,0:T(8,128)(2,1)S(1)}, f16[16,2176]{1,0:T(8,128)(2,1)S(1)}, u32[]{:S(2)}, u32[]{:S(2)}) %collective-permute-start.4) | collective-permute-done | bytes 69664 | tf_op jit(solution)/shard_map/ppermute | solution.py:43
  19.4 4.6 %attention.1.p0 = bf16[608,128]{1,0:T(8,128)(2,1)S(1)} custom-call(f32[16,2176]{1,0:T(8,128)S(1)} %add_add_fusion.q_ref, f32[4,16,128]{2,1,0:T(8,128)S(1)} %new_kv.1.kv_ref, bf16[16,2048,128]{2,1,0:T(8,128)(2,1)S(1)} %bitcast.10, bf16[16,2048,128]{2,1,0:T(8,128)(2,1)S(1)} %bitcast.13), custom_call_target="tpu_custom_call" | custom-call | flops 536870912 | bytes 16949248 | tf_op jit(solution)/shard_map/attention/pallas_call | solution.py:28
  24.1 1.4 %collective-permute-start.8 = (bf16[608,128]{1,0:T(8,128)(2,1)S(1)}, bf16[608,128]{1,0:T(8,128)(2,1)S(1)}, u32[]{:S(2)}, u32[]{:S(2)}) collective-permute-start(bf16[608,128]{1,0:T(8,128)(2,1)S(1)} %attention.1.p0), channel_id=1, source_target_pairs={{0,24},{8,16},{16,8},{24,0},{1,25},{9,17},{17,9},{25,1},{2,26},{10... | collective-permute-start | bytes 466952 | tf_op jit(solution)/shard_map/ppermute | solution.py:43
  25.9 1.5 %collective-permute-start.6 = (bf16[608,128]{1,0:T(8,128)(2,1)S(1)}, bf16[608,128]{1,0:T(8,128)(2,1)S(1)}, u32[]{:S(2)}, u32[]{:S(2)}) collective-permute-start(bf16[608,128]{1,0:T(8,128)(2,1)S(1)} %attention.1.p0), channel_id=1, source_target_pairs={{0,8},{8,0},{16,24},{24,16},{1,9},{9,1},{17,25},{25,17},{2,10},{10... | collective-permute-start | bytes 466952 | tf_op jit(solution)/shard_map/ppermute | solution.py:43
  27.4 2.0 %collective-permute-done.8.p3 = bf16[608,128]{1,0:T(8,128)(2,1)S(1)} collective-permute-done((bf16[608,128]{1,0:T(8,128)(2,1)S(1)}, bf16[608,128]{1,0:T(8,128)(2,1)S(1)}, u32[]{:S(2)}, u32[]{:S(2)}) %collective-permute-start.8) | collective-permute-done | bytes 155680 | tf_op jit(solution)/shard_map/ppermute | solution.py:43
  29.4 1.7 %collective-permute-done.7.p2 = bf16[608,128]{1,0:T(8,128)(2,1)S(1)} collective-permute-done((bf16[608,128]{1,0:T(8,128)(2,1)S(1)}, bf16[608,128]{1,0:T(8,128)(2,1)S(1)}, u32[]{:S(2)}, u32[]{:S(2)}) %collective-permute-start.7) | collective-permute-done | bytes 155680 | tf_op jit(solution)/shard_map/ppermute | solution.py:43
  32.2 2.0 %collective-permute-start.11 = (bf16[608,128]{1,0:T(8,128)(2,1)S(1)}, bf16[608,128]{1,0:T(8,128)(2,1)S(1)}, u32[]{:S(2)}, u32[]{:S(2)}) collective-permute-start(bf16[608,128]{1,0:T(8,128)(2,1)S(1)} %merge.1.p0), channel_id=1, source_target_pairs={{0,96},{32,64},{64,32},{96,0},{1,97},{33,65},{65,33},{97,1},{2,98}... | collective-permute-start | bytes 466952 | tf_op jit(solution)/shard_map/ppermute | solution.py:43
  35.5 2.5 %collective-permute-done.11.p3 = bf16[608,128]{1,0:T(8,128)(2,1)S(1)} collective-permute-done((bf16[608,128]{1,0:T(8,128)(2,1)S(1)}, bf16[608,128]{1,0:T(8,128)(2,1)S(1)}, u32[]{:S(2)}, u32[]{:S(2)}) %collective-permute-start.11) | collective-permute-done | bytes 155680 | tf_op jit(solution)/shard_map/ppermute | solution.py:43
  38.0 1.7 %collective-permute-done.10.p2 = bf16[608,128]{1,0:T(8,128)(2,1)S(1)} collective-permute-done((bf16[608,128]{1,0:T(8,128)(2,1)S(1)}, bf16[608,128]{1,0:T(8,128)(2,1)S(1)}, u32[]{:S(2)}, u32[]{:S(2)}) %collective-permute-start.10) | collective-permute-done | bytes 155680 | tf_op jit(solution)/shard_map/ppermute | solution.py:43
  39.9 1.5 %residual.1 = (bf16[16,256]{1,0:T(8,128)(2,1)S(1)}, f32[64,128]{1,0:T(8,128)S(1)}) custom-call(bf16[608,128]{1,0:T(8,128)(2,1)S(1)} %merge.1.p0, bf16[608,128]{1,0:T(8,128)(2,1)S(1)} %collective-permute-done.9.p1, bf16[608,128]{1,0:T(8,128)(2,1)S(1)} %collective-permute-done.10.p2, bf16[608,128]{1,0:T(8,128)(2,1)S(1)} %collective-permute-done.11.p3, ...), custom_call_target="tpu_custom_call" | custom-call | flops 16777216 | bytes 1688064 | tf_op jit(solution)/shard_map/residual/pallas_call | solution.py:28
  41.4 6.6 %collective-permute-start.12 = (bf16[16,256]{1,0:T(8,128)(2,1)S(1)}, bf16[16,256]{1,0:T(8,128)(2,1)S(1)}, u32[]{:S(2)}, u32[]{:S(2)}) collective-permute-start(bf16[16,256]{1,0:T(8,128)(2,1)S(1)} %get-tuple-element.11.res_ref), channel_id=1, source_target_pairs={{0,1},{1,0},{2,3},{3,2},{4,5},{5,4},{6,7},{7,6},{8,9},{9,8},{10,11... | collective-permute-start | bytes 24584 | tf_op jit(solution)/shard_map/ppermute | solution.py:361
  48.8 2.7 %collective-permute-start.15 = (bf16[2,16,256]{2,1,0:T(8,128)(2,1)S(1)}, bf16[2,16,256]{2,1,0:T(8,128)(2,1)S(1)}, u32[]{:S(2)}, u32[]{:S(2)}) collective-permute-start(bf16[2,16,256]{2,1,0:T(8,128)(2,1)S(1)} %pad_maximum_fusion.1.r0), channel_id=1, source_target_pairs={{0,6},{2,4},{4,2},{6,0},{1,7},{3,5},{5,3},{7,1},{8,14},{10,12},{12... | collective-permute-start | bytes 49160 | tf_op jit(solution)/shard_map/ppermute | solution.py:43
  52.6 3.0 %collective-permute-done.14.r2 = bf16[2,16,256]{2,1,0:T(8,128)(2,1)S(1)} collective-permute-done((bf16[2,16,256]{2,1,0:T(8,128)(2,1)S(1)}, bf16[2,16,256]{2,1,0:T(8,128)(2,1)S(1)}, u32[]{:S(2)}, u32[]{:S(2)}) %collective-permute-start.14) | collective-permute-done | bytes 16416 | tf_op jit(solution)/shard_map/ppermute | solution.py:43
  55.9 13.8 %all_to_all.10.in_ref = bf16[16,136,128]{2,1,0:T(8,128)(2,1)S(1)} all-to-all(bf16[16,136,128]{2,1,0:T(8,128)(2,1)S(1)} %up.1), channel_id=1, replica_groups=mesh['z'=4,'x'=4,'y'=4,'c'=2] {'z','x'}, dimensions={0} | all-to-all | bytes 1114112 | tf_op jit(solution)/shard_map/all_to_all | solution.py:49
  69.9 12.1 %all_to_all.11.act_ref = bf16[16,128,128]{2,1,0:T(8,128)(2,1)S(1)} all-to-all(bf16[16,128,128]{2,1,0:T(8,128)(2,1)S(1)} %act.1), channel_id=1, replica_groups=mesh['z'=4,'x'=4,'y'=4,'c'=2] {'z','x'}, dimensions={0} | all-to-all | bytes 1048576 | tf_op jit(solution)/shard_map/all_to_all | solution.py:49
  82.4 2.2 %collective-permute-start.17 = (bf16[2,16,256]{2,1,0:T(8,128)(2,1)S(1)}, bf16[2,16,256]{2,1,0:T(8,128)(2,1)S(1)}, u32[]{:S(2)}, u32[]{:S(2)}) collective-permute-start(bf16[2,16,256]{2,1,0:T(8,128)(2,1)S(1)} %get-tuple-element.14), channel_id=1, source_target_pairs={{0,4},{2,6},{4,0},{6,2},{1,5},{3,7},{5,1},{7,3},{8,12},{10,14},{12... | collective-permute-start | bytes 49160 | tf_op jit(solution)/shard_map/ppermute | solution.py:388
  84.6 1.6 %collective-permute-start.18 = (bf16[2,16,256]{2,1,0:T(8,128)(2,1)S(1)}, bf16[2,16,256]{2,1,0:T(8,128)(2,1)S(1)}, u32[]{:S(2)}, u32[]{:S(2)}) collective-permute-start(bf16[2,16,256]{2,1,0:T(8,128)(2,1)S(1)} %get-tuple-element.15), channel_id=1, source_target_pairs={{0,6},{2,4},{4,2},{6,0},{1,7},{3,5},{5,3},{7,1},{8,14},{10,12},{12... | collective-permute-start | bytes 49160 | tf_op jit(solution)/shard_map/ppermute | solution.py:388
  86.6 1.8 %collective-permute-done.18.d3 = bf16[2,16,256]{2,1,0:T(8,128)(2,1)S(1)} collective-permute-done((bf16[2,16,256]{2,1,0:T(8,128)(2,1)S(1)}, bf16[2,16,256]{2,1,0:T(8,128)(2,1)S(1)}, u32[]{:S(2)}, u32[]{:S(2)}) %collective-permute-start.18) | collective-permute-done | bytes 16416 | tf_op jit(solution)/shard_map/ppermute | solution.py:388
  88.5 5.4 %collective-permute-start.19 = (f32[16,256]{1,0:T(8,128)S(1)}, f32[16,256]{1,0:T(8,128)S(1)}, u32[]{:S(2)}, u32[]{:S(2)}) collective-permute-start(f32[16,256]{1,0:T(8,128)S(1)} %get-tuple-element.17), channel_id=1, source_target_pairs={{0,1},{1,0},{2,3},{3,2},{4,5},{5,4},{6,7},{7,6},{8,9},{9,8},{10,11... | collective-permute-start | bytes 49160 | tf_op jit(solution)/shard_map/ppermute | solution.py:409
  (66 shorter events, 13.0 us)
Async XLA Ops:
  2.3 6.2 %collective-permute-start.1 = (f16[16,2176]{1,0:T(8,128)(2,1)S(1)}, f16[16,2176]{1,0:T(8,128)(2,1)S(1)}, u32[]{:S(2)}, u32[]{:S(2)}) collective-permute-start(f16[16,2176]{1,0:T(8,128)(2,1)S(1)} %pad_maximum_fusion), channel_id=1, source_target_pairs={{0,64},{32,96},{64,0},{96,32},{1,65},{33,97},{65,1},{97,33},{2,66}... | collective-permute-start | bytes 208904 | tf_op jit(solution)/shard_map/ppermute | solution.py:43
  6.7 3.5 %collective-permute-start = (f16[16,2176]{1,0:T(8,128)(2,1)S(1)}, f16[16,2176]{1,0:T(8,128)(2,1)S(1)}, u32[]{:S(2)}, u32[]{:S(2)}) collective-permute-start(f16[16,2176]{1,0:T(8,128)(2,1)S(1)} %pad_maximum_fusion), channel_id=1, source_target_pairs={{0,32},{32,0},{64,96},{96,64},{1,33},{33,1},{65,97},{97,65},{2,34}... | collective-permute-start | bytes 208904 | tf_op jit(solution)/shard_map/ppermute | solution.py:43
  7.5 4.4 %collective-permute-start.2 = (f16[16,2176]{1,0:T(8,128)(2,1)S(1)}, f16[16,2176]{1,0:T(8,128)(2,1)S(1)}, u32[]{:S(2)}, u32[]{:S(2)}) collective-permute-start(f16[16,2176]{1,0:T(8,128)(2,1)S(1)} %pad_maximum_fusion), channel_id=1, source_target_pairs={{0,96},{32,64},{64,32},{96,0},{1,97},{33,65},{65,33},{97,1},{2,98}... | collective-permute-start | bytes 208904 | tf_op jit(solution)/shard_map/ppermute | solution.py:43
  11.9 6.1 %collective-permute-start.5 = (f16[16,2176]{1,0:T(8,128)(2,1)S(1)}, f16[16,2176]{1,0:T(8,128)(2,1)S(1)}, u32[]{:S(2)}, u32[]{:S(2)}) collective-permute-start(f16[16,2176]{1,0:T(8,128)(2,1)S(1)} %multiply_convert_fusion), channel_id=1, source_target_pairs={{0,24},{8,16},{16,8},{24,0},{1,25},{9,17},{17,9},{25,1},{2,26},{10... | collective-permute-start | bytes 208904 | tf_op jit(solution)/shard_map/ppermute | solution.py:43
  14.5 4.7 %collective-permute-start.4 = (f16[16,2176]{1,0:T(8,128)(2,1)S(1)}, f16[16,2176]{1,0:T(8,128)(2,1)S(1)}, u32[]{:S(2)}, u32[]{:S(2)}) collective-permute-start(f16[16,2176]{1,0:T(8,128)(2,1)S(1)} %multiply_convert_fusion), channel_id=1, source_target_pairs={{0,16},{8,24},{16,0},{24,8},{1,17},{9,25},{17,1},{25,9},{2,18},{10... | collective-permute-start | bytes 208904 | tf_op jit(solution)/shard_map/ppermute | solution.py:43
  15.0 4.2 %collective-permute-start.3 = (f16[16,2176]{1,0:T(8,128)(2,1)S(1)}, f16[16,2176]{1,0:T(8,128)(2,1)S(1)}, u32[]{:S(2)}, u32[]{:S(2)}) collective-permute-start(f16[16,2176]{1,0:T(8,128)(2,1)S(1)} %multiply_convert_fusion), channel_id=1, source_target_pairs={{0,8},{8,0},{16,24},{24,16},{1,9},{9,1},{17,25},{25,17},{2,10},{10... | collective-permute-start | bytes 208904 | tf_op jit(solution)/shard_map/ppermute | solution.py:43
  19.4 20.6 %copy-start.1 = (bf16[2048,256]{1,0:T(8,128)(2,1)S(1)}, bf16[2048,256]{1,0:T(8,128)(2,1)}, u32[]{:S(2)}) copy-start(bf16[2048,256]{1,0:T(8,128)(2,1)} %w_ref.3) | copy-start | bytes 3145732
  19.4 36.2 %copy-start.3 = (bf16[256,2048]{1,0:T(8,128)(2,1)S(1)}, bf16[256,2048]{1,0:T(8,128)(2,1)}, u32[]{:S(2)}) copy-start(bf16[256,2048]{1,0:T(8,128)(2,1)} %w_ref.4) | copy-start | bytes 3145732
  19.4 36.2 %copy-start.5 = (f32[256]{0:T(256)S(1)}, f32[256]{0:T(256)}, u32[]{:S(2)}) copy-start(f32[256]{0:T(256)} %param.23) | copy-start | bytes 3076
  19.4 62.6 %copy-start.2 = (bf16[2048,256]{1,0:T(8,128)(2,1)S(1)}, bf16[2048,256]{1,0:T(8,128)(2,1)}, u32[]{:S(2)}) copy-start(bf16[2048,256]{1,0:T(8,128)(2,1)} %w_ref.5) | copy-start | bytes 3145732
  24.1 5.4 %collective-permute-start.8 = (bf16[608,128]{1,0:T(8,128)(2,1)S(1)}, bf16[608,128]{1,0:T(8,128)(2,1)S(1)}, u32[]{:S(2)}, u32[]{:S(2)}) collective-permute-start(bf16[608,128]{1,0:T(8,128)(2,1)S(1)} %attention.1.p0), channel_id=1, source_target_pairs={{0,24},{8,16},{16,8},{24,0},{1,25},{9,17},{17,9},{25,1},{2,26},{10... | collective-permute-start | bytes 466952 | tf_op jit(solution)/shard_map/ppermute | solution.py:43
  25.4 5.7 %collective-permute-start.7 = (bf16[608,128]{1,0:T(8,128)(2,1)S(1)}, bf16[608,128]{1,0:T(8,128)(2,1)S(1)}, u32[]{:S(2)}, u32[]{:S(2)}) collective-permute-start(bf16[608,128]{1,0:T(8,128)(2,1)S(1)} %attention.1.p0), channel_id=1, source_target_pairs={{0,16},{8,24},{16,0},{24,8},{1,17},{9,25},{17,1},{25,9},{2,18},{10... | collective-permute-start | bytes 466952 | tf_op jit(solution)/shard_map/ppermute | solution.py:43
  25.9 5.7 %collective-permute-start.6 = (bf16[608,128]{1,0:T(8,128)(2,1)S(1)}, bf16[608,128]{1,0:T(8,128)(2,1)S(1)}, u32[]{:S(2)}, u32[]{:S(2)}) collective-permute-start(bf16[608,128]{1,0:T(8,128)(2,1)S(1)} %attention.1.p0), channel_id=1, source_target_pairs={{0,8},{8,0},{16,24},{24,16},{1,9},{9,1},{17,25},{25,17},{2,10},{10... | collective-permute-start | bytes 466952 | tf_op jit(solution)/shard_map/ppermute | solution.py:43
  32.2 5.8 %collective-permute-start.11 = (bf16[608,128]{1,0:T(8,128)(2,1)S(1)}, bf16[608,128]{1,0:T(8,128)(2,1)S(1)}, u32[]{:S(2)}, u32[]{:S(2)}) collective-permute-start(bf16[608,128]{1,0:T(8,128)(2,1)S(1)} %merge.1.p0), channel_id=1, source_target_pairs={{0,96},{32,64},{64,32},{96,0},{1,97},{33,65},{65,33},{97,1},{2,98}... | collective-permute-start | bytes 466952 | tf_op jit(solution)/shard_map/ppermute | solution.py:43
  34.1 5.6 %collective-permute-start.10 = (bf16[608,128]{1,0:T(8,128)(2,1)S(1)}, bf16[608,128]{1,0:T(8,128)(2,1)S(1)}, u32[]{:S(2)}, u32[]{:S(2)}) collective-permute-start(bf16[608,128]{1,0:T(8,128)(2,1)S(1)} %merge.1.p0), channel_id=1, source_target_pairs={{0,64},{32,96},{64,0},{96,32},{1,65},{33,97},{65,1},{97,33},{2,66}... | collective-permute-start | bytes 466952 | tf_op jit(solution)/shard_map/ppermute | solution.py:43
  34.5 5.3 %collective-permute-start.9 = (bf16[608,128]{1,0:T(8,128)(2,1)S(1)}, bf16[608,128]{1,0:T(8,128)(2,1)S(1)}, u32[]{:S(2)}, u32[]{:S(2)}) collective-permute-start(bf16[608,128]{1,0:T(8,128)(2,1)S(1)} %merge.1.p0), channel_id=1, source_target_pairs={{0,32},{32,0},{64,96},{96,64},{1,33},{33,1},{65,97},{97,65},{2,34}... | collective-permute-start | bytes 466952 | tf_op jit(solution)/shard_map/ppermute | solution.py:43
  41.4 7.4 %collective-permute-start.12 = (bf16[16,256]{1,0:T(8,128)(2,1)S(1)}, bf16[16,256]{1,0:T(8,128)(2,1)S(1)}, u32[]{:S(2)}, u32[]{:S(2)}) collective-permute-start(bf16[16,256]{1,0:T(8,128)(2,1)S(1)} %get-tuple-element.11.res_ref), channel_id=1, source_target_pairs={{0,1},{1,0},{2,3},{3,2},{4,5},{5,4},{6,7},{7,6},{8,9},{9,8},{10,11... | collective-permute-start | bytes 24584 | tf_op jit(solution)/shard_map/ppermute | solution.py:361
  48.8 3.9 %collective-permute-start.15 = (bf16[2,16,256]{2,1,0:T(8,128)(2,1)S(1)}, bf16[2,16,256]{2,1,0:T(8,128)(2,1)S(1)}, u32[]{:S(2)}, u32[]{:S(2)}) collective-permute-start(bf16[2,16,256]{2,1,0:T(8,128)(2,1)S(1)} %pad_maximum_fusion.1.r0), channel_id=1, source_target_pairs={{0,6},{2,4},{4,2},{6,0},{1,7},{3,5},{5,3},{7,1},{8,14},{10,12},{12... | collective-permute-start | bytes 49160 | tf_op jit(solution)/shard_map/ppermute | solution.py:43
  51.5 4.1 %collective-permute-start.14 = (bf16[2,16,256]{2,1,0:T(8,128)(2,1)S(1)}, bf16[2,16,256]{2,1,0:T(8,128)(2,1)S(1)}, u32[]{:S(2)}, u32[]{:S(2)}) collective-permute-start(bf16[2,16,256]{2,1,0:T(8,128)(2,1)S(1)} %pad_maximum_fusion.1.r0), channel_id=1, source_target_pairs={{0,4},{2,6},{4,0},{6,2},{1,5},{3,7},{5,1},{7,3},{8,12},{10,14},{12... | collective-permute-start | bytes 49160 | tf_op jit(solution)/shard_map/ppermute | solution.py:43
  51.9 3.7 %collective-permute-start.13 = (bf16[2,16,256]{2,1,0:T(8,128)(2,1)S(1)}, bf16[2,16,256]{2,1,0:T(8,128)(2,1)S(1)}, u32[]{:S(2)}, u32[]{:S(2)}) collective-permute-start(bf16[2,16,256]{2,1,0:T(8,128)(2,1)S(1)} %pad_maximum_fusion.1.r0), channel_id=1, source_target_pairs={{0,2},{2,0},{4,6},{6,4},{1,3},{3,1},{5,7},{7,5},{8,10},{10,8},{12,... | collective-permute-start | bytes 49160 | tf_op jit(solution)/shard_map/ppermute | solution.py:43
  82.3 3.9 %collective-permute-start.16 = (bf16[2,16,256]{2,1,0:T(8,128)(2,1)S(1)}, bf16[2,16,256]{2,1,0:T(8,128)(2,1)S(1)}, u32[]{:S(2)}, u32[]{:S(2)}) collective-permute-start(bf16[2,16,256]{2,1,0:T(8,128)(2,1)S(1)} %get-tuple-element.13), channel_id=1, source_target_pairs={{0,2},{2,0},{4,6},{6,4},{1,3},{3,1},{5,7},{7,5},{8,10},{10,8},{12,... | collective-permute-start | bytes 49160 | tf_op jit(solution)/shard_map/ppermute | solution.py:388
  82.4 4.2 %collective-permute-start.17 = (bf16[2,16,256]{2,1,0:T(8,128)(2,1)S(1)}, bf16[2,16,256]{2,1,0:T(8,128)(2,1)S(1)}, u32[]{:S(2)}, u32[]{:S(2)}) collective-permute-start(bf16[2,16,256]{2,1,0:T(8,128)(2,1)S(1)} %get-tuple-element.14), channel_id=1, source_target_pairs={{0,4},{2,6},{4,0},{6,2},{1,5},{3,7},{5,1},{7,3},{8,12},{10,14},{12... | collective-permute-start | bytes 49160 | tf_op jit(solution)/shard_map/ppermute | solution.py:388
  84.6 3.8 %collective-permute-start.18 = (bf16[2,16,256]{2,1,0:T(8,128)(2,1)S(1)}, bf16[2,16,256]{2,1,0:T(8,128)(2,1)S(1)}, u32[]{:S(2)}, u32[]{:S(2)}) collective-permute-start(bf16[2,16,256]{2,1,0:T(8,128)(2,1)S(1)} %get-tuple-element.15), channel_id=1, source_target_pairs={{0,6},{2,4},{4,2},{6,0},{1,7},{3,5},{5,3},{7,1},{8,14},{10,12},{12... | collective-permute-start | bytes 49160 | tf_op jit(solution)/shard_map/ppermute | solution.py:388
  88.5 6.2 %collective-permute-start.19 = (f32[16,256]{1,0:T(8,128)S(1)}, f32[16,256]{1,0:T(8,128)S(1)}, u32[]{:S(2)}, u32[]{:S(2)}) collective-permute-start(f32[16,256]{1,0:T(8,128)S(1)} %get-tuple-element.17), channel_id=1, source_target_pairs={{0,1},{1,0},{2,3},{3,2},{4,5},{5,4},{6,7},{7,6},{8,9},{9,8},{10,11... | collective-permute-start | bytes 49160 | tf_op jit(solution)/shard_map/ppermute | solution.py:409
  (10 other events, 95.1 us)

commit v5 on v4

--- a/solution.py
+++ b/solution.py
@@ -60,22 +60,21 @@
     return hi, mid, lo
 
 
-def new_kv_body(scaled_ref, wk_ref, wv_ref, kv_ref):
-    at = 0
-    for w in (wk_ref, wv_ref):
-        part = dot(scaled_ref[...], w[...])
-        for t in range(part.shape[1] // LANES):
-            kv_ref[at] = part[:, t * LANES : (t + 1) * LANES]
-            at += 1
-
-
-def attention_body(width, q_ref, kv_ref, k_ref, v_ref, out_ref, q_scr, s_scr):
+def hold_body(in_ref, out_ref):
+    out_ref[...] = in_ref[...]
+
+
+def attention_body(width, q_ref, scaled_ref, wk_ref, wv_ref, k_ref, v_ref, out_ref, q_scr, s_scr):
     rows, spots, _ = k_ref.shape
     heads = q_ref.shape[1] // LANES - 1
     inv = lax.rsqrt(q_ref[:, heads * LANES :] * (32.0 / width) + EPS)
     rest = rows * 2 * heads + 2 * heads
-    for t in range(kv_ref.shape[0]):
-        out_ref[rest + t * rows : rest + (t + 1) * rows] = (kv_ref[t] * inv).astype(BF16)
+    for w in (wk_ref, wv_ref):
+        part = dot(scaled_ref[...], w[...])
+        for t in range(part.shape[1] // LANES):
+            tile = part[:, t * LANES : (t + 1) * LANES] * inv
+            out_ref[rest : rest + rows] = tile.astype(BF16)
+            rest += rows
     for h in range(heads):
         part = q_ref[:, h * LANES : (h + 1) * LANES] * 0.125 * inv
         q_scr[h * rows : (h + 1) * rows] = part.astype(BF16).astype(F32) * 0.125
@@ -304,13 +303,11 @@
     query = dot(scaled, w_query) * 32.0
     spread = jnp.broadcast_to(squares * 0.125, (rows, LANES))
     q_part = jnp.concatenate([query, spread], axis=1)
-    kv_part = local_call(
-        new_kv_body,
-        "new_kv",
-        struct((4, rows, LANES), F32),
+    held = local_call(
+        hold_body,
+        "hold",
+        struct(scaled.shape, BF16),
         scaled,
-        w_key,
-        w_value,
         flops=1 << 33,
     )
     q_part = q_part.astype(jnp.float16)
@@ -324,7 +321,9 @@
         "attention",
         struct((packed, LANES), BF16),
         total_q,
-        kv_part,
+        held,
+        w_key,
+        w_value,
         cache_keys.reshape(rows, spots, LANES),
         cache_values.reshape(rows, spots, LANES),
         flops=4 * rows * vecs * spots * LANES,

time: 95.5 us -> 95.4 us (level)
  waiting for transfers between devices: 21.5 us -> 24.3 us
  local copies, waits for them, and re-layouts: 3.15 us -> 0.57 us
    ppermute x15, waiting for transfers between devices: 17.7 us -> 20.5 us  [from_peers(): lax.ppermute(shard, axis, [(i, i ^ k) for i in range(peers)])]
    unnamed x28, local copies, waits for them, and re-layouts: 3 us -> 0.42 us
where the time goes in v5:
time: 95.4 us; the launch traced here: 95.2 us
  starting transfers between devices  34.4 us (36%)
  blocking collectives  25.9 us (27%)
  waiting for transfers between devices  24.3 us (25%)
  Pallas kernels  7.88 us (8%)
  other arithmetic  1.03 us (1%)
    all_to_all x2, blocking collectives, exchanged(): return lax.all_to_all(tiles, axis, 0, 0, tiled=True)  25.9 us
    ppermute x15, waiting for transfers between devices, from_peers(): lax.ppermute(shard, axis, [(i, i ^ k) for i in range(peers)])  20.5 us
    ppermute x15, starting transfers between devices, from_peers(): lax.ppermute(shard, axis, [(i, i ^ k) for i in range(peers)])  18.6 us
    pallas_call x9, Pallas kernels, local_call(): pl.pallas_call(body, name=name, out_shape=outs, in_specs=[HBM if i in far...  7.88 us
    ppermute x1, starting transfers between devices, shards(): pair = jnp.stack([residual, lax.ppermute(residual, 'c', [(0, 1), (1, 0)])])  6.58 us
    ppermute x1, starting transfers between devices, shards(): lax.ppermute(other, 'c', [(0, 1), (1, 0)])  5.37 us
    ppermute x3, starting transfers between devices, shards(): lax.ppermute(d, 'y', [(i, i ^ k) for i in range(4)])  3.93 us
    ppermute x3, waiting for transfers between devices, shards(): lax.ppermute(d, 'y', [(i, i ^ k) for i in range(4)])  2.18 us
  transfers between devices with their start and end apart: 20, of which 16 were waited for; matrix products, arithmetic and copies ran while one was open for 0% of the time, Pallas kernels for 0%

profile of v5, /device:TPU:1, one launch (start us, length us, event | category | flops | bytes accessed | tf_op | source)
XLA Modules:
  0.0 95.2 jit_solution(18180770170365262424)
XLA Ops:
  2.3 4.5 %collective-permute-start.1 = (f16[16,2176]{1,0:T(8,128)(2,1)S(1)}, f16[16,2176]{1,0:T(8,128)(2,1)S(1)}, u32[]{:S(2)}, u32[]{:S(2)}) collective-permute-start(f16[16,2176]{1,0:T(8,128)(2,1)S(1)} %pad_maximum_fusion), channel_id=1, source_target_pairs={{0,64},{32,96},{64,0},{96,32},{1,65},{33,97},{65,1},{97,33},{2,66}... | collective-permute-start | bytes 208904 | tf_op jit(solution)/shard_map/ppermute | solution.py:43
  8.4 1.8 %collective-permute-done = f16[16,2176]{1,0:T(8,128)(2,1)S(1)} collective-permute-done((f16[16,2176]{1,0:T(8,128)(2,1)S(1)}, f16[16,2176]{1,0:T(8,128)(2,1)S(1)}, u32[]{:S(2)}, u32[]{:S(2)}) %collective-permute-start) | collective-permute-done | bytes 69664 | tf_op jit(solution)/shard_map/ppermute | solution.py:43
  10.3 1.6 %collective-permute-done.2 = f16[16,2176]{1,0:T(8,128)(2,1)S(1)} collective-permute-done((f16[16,2176]{1,0:T(8,128)(2,1)S(1)}, f16[16,2176]{1,0:T(8,128)(2,1)S(1)}, u32[]{:S(2)}, u32[]{:S(2)}) %collective-permute-start.2) | collective-permute-done | bytes 69664 | tf_op jit(solution)/shard_map/ppermute | solution.py:43
  12.0 2.6 %collective-permute-start.5 = (f16[16,2176]{1,0:T(8,128)(2,1)S(1)}, f16[16,2176]{1,0:T(8,128)(2,1)S(1)}, u32[]{:S(2)}, u32[]{:S(2)}) collective-permute-start(f16[16,2176]{1,0:T(8,128)(2,1)S(1)} %multiply_convert_fusion), channel_id=1, source_target_pairs={{0,24},{8,16},{16,8},{24,0},{1,25},{9,17},{17,9},{25,1},{2,26},{10... | collective-permute-start | bytes 208904 | tf_op jit(solution)/shard_map/ppermute | solution.py:43
  15.3 1.1 %collective-permute-done.5 = f16[16,2176]{1,0:T(8,128)(2,1)S(1)} collective-permute-done((f16[16,2176]{1,0:T(8,128)(2,1)S(1)}, f16[16,2176]{1,0:T(8,128)(2,1)S(1)}, u32[]{:S(2)}, u32[]{:S(2)}) %collective-permute-start.5) | collective-permute-done | bytes 69664 | tf_op jit(solution)/shard_map/ppermute | solution.py:43
  16.4 2.8 %collective-permute-done.4 = f16[16,2176]{1,0:T(8,128)(2,1)S(1)} collective-permute-done((f16[16,2176]{1,0:T(8,128)(2,1)S(1)}, f16[16,2176]{1,0:T(8,128)(2,1)S(1)}, u32[]{:S(2)}, u32[]{:S(2)}) %collective-permute-start.4) | collective-permute-done | bytes 69664 | tf_op jit(solution)/shard_map/ppermute | solution.py:43
  19.5 4.5 %attention.1.p0 = bf16[608,128]{1,0:T(8,128)(2,1)S(1)} custom-call(f32[16,2176]{1,0:T(8,128)S(1)} %add_add_fusion.q_ref, bf16[16,256]{1,0:T(8,128)(2,1)S(1)} %hold.1.scaled_ref, bf16[256,256]{1,0:T(8,128)(2,1)S(1)} %copy-done.4, bf16[256,256]{1,0:T(8,128)(2,1)S(1)} %copy-done.5, bf16[16,2048,128]{2,1,0:T(8,128)(2,1)S(1)} %bitcast.10, ...), custom_call_target="tpu_custom_call" | custom-call | flops 536870912 | bytes 17186816 | tf_op jit(solution)/shard_map/attention/pallas_call | solution.py:28
  24.0 1.0 %collective-permute-start.8 = (bf16[608,128]{1,0:T(8,128)(2,1)S(1)}, bf16[608,128]{1,0:T(8,128)(2,1)S(1)}, u32[]{:S(2)}, u32[]{:S(2)}) collective-permute-start(bf16[608,128]{1,0:T(8,128)(2,1)S(1)} %attention.1.p0), channel_id=1, source_target_pairs={{0,24},{8,16},{16,8},{24,0},{1,25},{9,17},{17,9},{25,1},{2,26},{10... | collective-permute-start | bytes 466952 | tf_op jit(solution)/shard_map/ppermute | solution.py:43
  25.8 1.5 %collective-permute-start.6 = (bf16[608,128]{1,0:T(8,128)(2,1)S(1)}, bf16[608,128]{1,0:T(8,128)(2,1)S(1)}, u32[]{:S(2)}, u32[]{:S(2)}) collective-permute-start(bf16[608,128]{1,0:T(8,128)(2,1)S(1)} %attention.1.p0), channel_id=1, source_target_pairs={{0,8},{8,0},{16,24},{24,16},{1,9},{9,1},{17,25},{25,17},{2,10},{10... | collective-permute-start | bytes 466952 | tf_op jit(solution)/shard_map/ppermute | solution.py:43
  27.3 3.7 %collective-permute-done.8.p3 = bf16[608,128]{1,0:T(8,128)(2,1)S(1)} collective-permute-done((bf16[608,128]{1,0:T(8,128)(2,1)S(1)}, bf16[608,128]{1,0:T(8,128)(2,1)S(1)}, u32[]{:S(2)}, u32[]{:S(2)}) %collective-permute-start.8) | collective-permute-done | bytes 155680 | tf_op jit(solution)/shard_map/ppermute | solution.py:43
  32.1 2.0 %collective-permute-start.11 = (bf16[608,128]{1,0:T(8,128)(2,1)S(1)}, bf16[608,128]{1,0:T(8,128)(2,1)S(1)}, u32[]{:S(2)}, u32[]{:S(2)}) collective-permute-start(bf16[608,128]{1,0:T(8,128)(2,1)S(1)} %merge.1.p0), channel_id=1, source_target_pairs={{0,96},{32,64},{64,32},{96,0},{1,97},{33,65},{65,33},{97,1},{2,98}... | collective-permute-start | bytes 466952 | tf_op jit(solution)/shard_map/ppermute | solution.py:43
  34.4 1.0 %collective-permute-start.9 = (bf16[608,128]{1,0:T(8,128)(2,1)S(1)}, bf16[608,128]{1,0:T(8,128)(2,1)S(1)}, u32[]{:S(2)}, u32[]{:S(2)}) collective-permute-start(bf16[608,128]{1,0:T(8,128)(2,1)S(1)} %merge.1.p0), channel_id=1, source_target_pairs={{0,32},{32,0},{64,96},{96,64},{1,33},{33,1},{65,97},{97,65},{2,34}... | collective-permute-start | bytes 466952 | tf_op jit(solution)/shard_map/ppermute | solution.py:43
  35.4 2.5 %collective-permute-done.11.p3 = bf16[608,128]{1,0:T(8,128)(2,1)S(1)} collective-permute-done((bf16[608,128]{1,0:T(8,128)(2,1)S(1)}, bf16[608,128]{1,0:T(8,128)(2,1)S(1)}, u32[]{:S(2)}, u32[]{:S(2)}) %collective-permute-start.11) | collective-permute-done | bytes 155680 | tf_op jit(solution)/shard_map/ppermute | solution.py:43
  37.9 1.7 %collective-permute-done.10.p2 = bf16[608,128]{1,0:T(8,128)(2,1)S(1)} collective-permute-done((bf16[608,128]{1,0:T(8,128)(2,1)S(1)}, bf16[608,128]{1,0:T(8,128)(2,1)S(1)}, u32[]{:S(2)}, u32[]{:S(2)}) %collective-permute-start.10) | collective-permute-done | bytes 155680 | tf_op jit(solution)/shard_map/ppermute | solution.py:43
  39.8 1.5 %residual.1 = (bf16[16,256]{1,0:T(8,128)(2,1)S(1)}, f32[64,128]{1,0:T(8,128)S(1)}) custom-call(bf16[608,128]{1,0:T(8,128)(2,1)S(1)} %merge.1.p0, bf16[608,128]{1,0:T(8,128)(2,1)S(1)} %collective-permute-done.9.p1, bf16[608,128]{1,0:T(8,128)(2,1)S(1)} %collective-permute-done.10.p2, bf16[608,128]{1,0:T(8,128)(2,1)S(1)} %collective-permute-done.11.p3, ...), custom_call_target="tpu_custom_call" | custom-call | flops 16777216 | bytes 1688064 | tf_op jit(solution)/shard_map/residual/pallas_call | solution.py:28
  41.3 6.6 %collective-permute-start.12 = (bf16[16,256]{1,0:T(8,128)(2,1)S(1)}, bf16[16,256]{1,0:T(8,128)(2,1)S(1)}, u32[]{:S(2)}, u32[]{:S(2)}) collective-permute-start(bf16[16,256]{1,0:T(8,128)(2,1)S(1)} %get-tuple-element.11.res_ref), channel_id=1, source_target_pairs={{0,1},{1,0},{2,3},{3,2},{4,5},{5,4},{6,7},{7,6},{8,9},{9,8},{10,11... | collective-permute-start | bytes 24584 | tf_op jit(solution)/shard_map/ppermute | solution.py:360
  48.7 2.7 %collective-permute-start.15 = (bf16[2,16,256]{2,1,0:T(8,128)(2,1)S(1)}, bf16[2,16,256]{2,1,0:T(8,128)(2,1)S(1)}, u32[]{:S(2)}, u32[]{:S(2)}) collective-permute-start(bf16[2,16,256]{2,1,0:T(8,128)(2,1)S(1)} %pad_maximum_fusion.1.r0), channel_id=1, source_target_pairs={{0,6},{2,4},{4,2},{6,0},{1,7},{3,5},{5,3},{7,1},{8,14},{10,12},{12... | collective-permute-start | bytes 49160 | tf_op jit(solution)/shard_map/ppermute | solution.py:43
  52.6 3.0 %collective-permute-done.14.r2 = bf16[2,16,256]{2,1,0:T(8,128)(2,1)S(1)} collective-permute-done((bf16[2,16,256]{2,1,0:T(8,128)(2,1)S(1)}, bf16[2,16,256]{2,1,0:T(8,128)(2,1)S(1)}, u32[]{:S(2)}, u32[]{:S(2)}) %collective-permute-start.14) | collective-permute-done | bytes 16416 | tf_op jit(solution)/shard_map/ppermute | solution.py:43
  55.9 13.8 %all_to_all.10.in_ref = bf16[16,136,128]{2,1,0:T(8,128)(2,1)S(1)} all-to-all(bf16[16,136,128]{2,1,0:T(8,128)(2,1)S(1)} %up.1), channel_id=1, replica_groups=mesh['z'=4,'x'=4,'y'=4,'c'=2] {'z','x'}, dimensions={0} | all-to-all | bytes 1114112 | tf_op jit(solution)/shard_map/all_to_all | solution.py:49
  69.8 12.1 %all_to_all.11.act_ref = bf16[16,128,128]{2,1,0:T(8,128)(2,1)S(1)} all-to-all(bf16[16,128,128]{2,1,0:T(8,128)(2,1)S(1)} %act.1), channel_id=1, replica_groups=mesh['z'=4,'x'=4,'y'=4,'c'=2] {'z','x'}, dimensions={0} | all-to-all | bytes 1048576 | tf_op jit(solution)/shard_map/all_to_all | solution.py:49
  82.3 2.2 %collective-permute-start.17 = (bf16[2,16,256]{2,1,0:T(8,128)(2,1)S(1)}, bf16[2,16,256]{2,1,0:T(8,128)(2,1)S(1)}, u32[]{:S(2)}, u32[]{:S(2)}) collective-permute-start(bf16[2,16,256]{2,1,0:T(8,128)(2,1)S(1)} %get-tuple-element.14), channel_id=1, source_target_pairs={{0,4},{2,6},{4,0},{6,2},{1,5},{3,7},{5,1},{7,3},{8,12},{10,14},{12... | collective-permute-start | bytes 49160 | tf_op jit(solution)/shard_map/ppermute | solution.py:387
  84.6 1.6 %collective-permute-start.18 = (bf16[2,16,256]{2,1,0:T(8,128)(2,1)S(1)}, bf16[2,16,256]{2,1,0:T(8,128)(2,1)S(1)}, u32[]{:S(2)}, u32[]{:S(2)}) collective-permute-start(bf16[2,16,256]{2,1,0:T(8,128)(2,1)S(1)} %get-tuple-element.15), channel_id=1, source_target_pairs={{0,6},{2,4},{4,2},{6,0},{1,7},{3,5},{5,3},{7,1},{8,14},{10,12},{12... | collective-permute-start | bytes 49160 | tf_op jit(solution)/shard_map/ppermute | solution.py:387
  86.5 1.9 %collective-permute-done.18.d3 = bf16[2,16,256]{2,1,0:T(8,128)(2,1)S(1)} collective-permute-done((bf16[2,16,256]{2,1,0:T(8,128)(2,1)S(1)}, bf16[2,16,256]{2,1,0:T(8,128)(2,1)S(1)}, u32[]{:S(2)}, u32[]{:S(2)}) %collective-permute-start.18) | collective-permute-done | bytes 16416 | tf_op jit(solution)/shard_map/ppermute | solution.py:387
  88.4 5.4 %collective-permute-start.19 = (f32[16,256]{1,0:T(8,128)S(1)}, f32[16,256]{1,0:T(8,128)S(1)}, u32[]{:S(2)}, u32[]{:S(2)}) collective-permute-start(f32[16,256]{1,0:T(8,128)S(1)} %get-tuple-element.17), channel_id=1, source_target_pairs={{0,1},{1,0},{2,3},{3,2},{4,5},{5,4},{6,7},{7,6},{8,9},{9,8},{10,11... | collective-permute-start | bytes 49160 | tf_op jit(solution)/shard_map/ppermute | solution.py:408
  (66 shorter events, 11.3 us)
Async XLA Ops:
  2.3 6.2 %collective-permute-start.1 = (f16[16,2176]{1,0:T(8,128)(2,1)S(1)}, f16[16,2176]{1,0:T(8,128)(2,1)S(1)}, u32[]{:S(2)}, u32[]{:S(2)}) collective-permute-start(f16[16,2176]{1,0:T(8,128)(2,1)S(1)} %pad_maximum_fusion), channel_id=1, source_target_pairs={{0,64},{32,96},{64,0},{96,32},{1,65},{33,97},{65,1},{97,33},{2,66}... | collective-permute-start | bytes 208904 | tf_op jit(solution)/shard_map/ppermute | solution.py:43
  6.7 3.5 %collective-permute-start = (f16[16,2176]{1,0:T(8,128)(2,1)S(1)}, f16[16,2176]{1,0:T(8,128)(2,1)S(1)}, u32[]{:S(2)}, u32[]{:S(2)}) collective-permute-start(f16[16,2176]{1,0:T(8,128)(2,1)S(1)} %pad_maximum_fusion), channel_id=1, source_target_pairs={{0,32},{32,0},{64,96},{96,64},{1,33},{33,1},{65,97},{97,65},{2,34}... | collective-permute-start | bytes 208904 | tf_op jit(solution)/shard_map/ppermute | solution.py:43
  7.5 4.4 %collective-permute-start.2 = (f16[16,2176]{1,0:T(8,128)(2,1)S(1)}, f16[16,2176]{1,0:T(8,128)(2,1)S(1)}, u32[]{:S(2)}, u32[]{:S(2)}) collective-permute-start(f16[16,2176]{1,0:T(8,128)(2,1)S(1)} %pad_maximum_fusion), channel_id=1, source_target_pairs={{0,96},{32,64},{64,32},{96,0},{1,97},{33,65},{65,33},{97,1},{2,98}... | collective-permute-start | bytes 208904 | tf_op jit(solution)/shard_map/ppermute | solution.py:43
  12.0 4.5 %collective-permute-start.5 = (f16[16,2176]{1,0:T(8,128)(2,1)S(1)}, f16[16,2176]{1,0:T(8,128)(2,1)S(1)}, u32[]{:S(2)}, u32[]{:S(2)}) collective-permute-start(f16[16,2176]{1,0:T(8,128)(2,1)S(1)} %multiply_convert_fusion), channel_id=1, source_target_pairs={{0,24},{8,16},{16,8},{24,0},{1,25},{9,17},{17,9},{25,1},{2,26},{10... | collective-permute-start | bytes 208904 | tf_op jit(solution)/shard_map/ppermute | solution.py:43
  14.5 4.7 %collective-permute-start.4 = (f16[16,2176]{1,0:T(8,128)(2,1)S(1)}, f16[16,2176]{1,0:T(8,128)(2,1)S(1)}, u32[]{:S(2)}, u32[]{:S(2)}) collective-permute-start(f16[16,2176]{1,0:T(8,128)(2,1)S(1)} %multiply_convert_fusion), channel_id=1, source_target_pairs={{0,16},{8,24},{16,0},{24,8},{1,17},{9,25},{17,1},{25,9},{2,18},{10... | collective-permute-start | bytes 208904 | tf_op jit(solution)/shard_map/ppermute | solution.py:43
  15.1 4.2 %collective-permute-start.3 = (f16[16,2176]{1,0:T(8,128)(2,1)S(1)}, f16[16,2176]{1,0:T(8,128)(2,1)S(1)}, u32[]{:S(2)}, u32[]{:S(2)}) collective-permute-start(f16[16,2176]{1,0:T(8,128)(2,1)S(1)} %multiply_convert_fusion), channel_id=1, source_target_pairs={{0,8},{8,0},{16,24},{24,16},{1,9},{9,1},{17,25},{25,17},{2,10},{10... | collective-permute-start | bytes 208904 | tf_op jit(solution)/shard_map/ppermute | solution.py:43
  19.4 20.4 %copy-start.1 = (bf16[2048,256]{1,0:T(8,128)(2,1)S(1)}, bf16[2048,256]{1,0:T(8,128)(2,1)}, u32[]{:S(2)}) copy-start(bf16[2048,256]{1,0:T(8,128)(2,1)} %w_ref.3) | copy-start | bytes 3145732
  19.4 36.1 %copy-start.3 = (bf16[256,2048]{1,0:T(8,128)(2,1)S(1)}, bf16[256,2048]{1,0:T(8,128)(2,1)}, u32[]{:S(2)}) copy-start(bf16[256,2048]{1,0:T(8,128)(2,1)} %w_ref.4) | copy-start | bytes 3145732
  19.4 36.1 %copy-start.7 = (f32[256]{0:T(256)S(1)}, f32[256]{0:T(256)}, u32[]{:S(2)}) copy-start(f32[256]{0:T(256)} %param.23) | copy-start | bytes 3076
  19.5 62.5 %copy-start.2 = (bf16[2048,256]{1,0:T(8,128)(2,1)S(1)}, bf16[2048,256]{1,0:T(8,128)(2,1)}, u32[]{:S(2)}) copy-start(bf16[2048,256]{1,0:T(8,128)(2,1)} %w_ref.5) | copy-start | bytes 3145732
  24.0 7.0 %collective-permute-start.8 = (bf16[608,128]{1,0:T(8,128)(2,1)S(1)}, bf16[608,128]{1,0:T(8,128)(2,1)S(1)}, u32[]{:S(2)}, u32[]{:S(2)}) collective-permute-start(bf16[608,128]{1,0:T(8,128)(2,1)S(1)} %attention.1.p0), channel_id=1, source_target_pairs={{0,24},{8,16},{16,8},{24,0},{1,25},{9,17},{17,9},{25,1},{2,26},{10... | collective-permute-start | bytes 466952 | tf_op jit(solution)/shard_map/ppermute | solution.py:43
  25.0 6.0 %collective-permute-start.7 = (bf16[608,128]{1,0:T(8,128)(2,1)S(1)}, bf16[608,128]{1,0:T(8,128)(2,1)S(1)}, u32[]{:S(2)}, u32[]{:S(2)}) collective-permute-start(bf16[608,128]{1,0:T(8,128)(2,1)S(1)} %attention.1.p0), channel_id=1, source_target_pairs={{0,16},{8,24},{16,0},{24,8},{1,17},{9,25},{17,1},{25,9},{2,18},{10... | collective-permute-start | bytes 466952 | tf_op jit(solution)/shard_map/ppermute | solution.py:43
  25.8 5.8 %collective-permute-start.6 = (bf16[608,128]{1,0:T(8,128)(2,1)S(1)}, bf16[608,128]{1,0:T(8,128)(2,1)S(1)}, u32[]{:S(2)}, u32[]{:S(2)}) collective-permute-start(bf16[608,128]{1,0:T(8,128)(2,1)S(1)} %attention.1.p0), channel_id=1, source_target_pairs={{0,8},{8,0},{16,24},{24,16},{1,9},{9,1},{17,25},{25,17},{2,10},{10... | collective-permute-start | bytes 466952 | tf_op jit(solution)/shard_map/ppermute | solution.py:43
  32.1 5.8 %collective-permute-start.11 = (bf16[608,128]{1,0:T(8,128)(2,1)S(1)}, bf16[608,128]{1,0:T(8,128)(2,1)S(1)}, u32[]{:S(2)}, u32[]{:S(2)}) collective-permute-start(bf16[608,128]{1,0:T(8,128)(2,1)S(1)} %merge.1.p0), channel_id=1, source_target_pairs={{0,96},{32,64},{64,32},{96,0},{1,97},{33,65},{65,33},{97,1},{2,98}... | collective-permute-start | bytes 466952 | tf_op jit(solution)/shard_map/ppermute | solution.py:43
  34.0 5.6 %collective-permute-start.10 = (bf16[608,128]{1,0:T(8,128)(2,1)S(1)}, bf16[608,128]{1,0:T(8,128)(2,1)S(1)}, u32[]{:S(2)}, u32[]{:S(2)}) collective-permute-start(bf16[608,128]{1,0:T(8,128)(2,1)S(1)} %merge.1.p0), channel_id=1, source_target_pairs={{0,64},{32,96},{64,0},{96,32},{1,65},{33,97},{65,1},{97,33},{2,66}... | collective-permute-start | bytes 466952 | tf_op jit(solution)/shard_map/ppermute | solution.py:43
  34.4 5.3 %collective-permute-start.9 = (bf16[608,128]{1,0:T(8,128)(2,1)S(1)}, bf16[608,128]{1,0:T(8,128)(2,1)S(1)}, u32[]{:S(2)}, u32[]{:S(2)}) collective-permute-start(bf16[608,128]{1,0:T(8,128)(2,1)S(1)} %merge.1.p0), channel_id=1, source_target_pairs={{0,32},{32,0},{64,96},{96,64},{1,33},{33,1},{65,97},{97,65},{2,34}... | collective-permute-start | bytes 466952 | tf_op jit(solution)/shard_map/ppermute | solution.py:43
  41.3 7.4 %collective-permute-start.12 = (bf16[16,256]{1,0:T(8,128)(2,1)S(1)}, bf16[16,256]{1,0:T(8,128)(2,1)S(1)}, u32[]{:S(2)}, u32[]{:S(2)}) collective-permute-start(bf16[16,256]{1,0:T(8,128)(2,1)S(1)} %get-tuple-element.11.res_ref), channel_id=1, source_target_pairs={{0,1},{1,0},{2,3},{3,2},{4,5},{5,4},{6,7},{7,6},{8,9},{9,8},{10,11... | collective-permute-start | bytes 24584 | tf_op jit(solution)/shard_map/ppermute | solution.py:360
  48.7 3.9 %collective-permute-start.15 = (bf16[2,16,256]{2,1,0:T(8,128)(2,1)S(1)}, bf16[2,16,256]{2,1,0:T(8,128)(2,1)S(1)}, u32[]{:S(2)}, u32[]{:S(2)}) collective-permute-start(bf16[2,16,256]{2,1,0:T(8,128)(2,1)S(1)} %pad_maximum_fusion.1.r0), channel_id=1, source_target_pairs={{0,6},{2,4},{4,2},{6,0},{1,7},{3,5},{5,3},{7,1},{8,14},{10,12},{12... | collective-permute-start | bytes 49160 | tf_op jit(solution)/shard_map/ppermute | solution.py:43
  51.4 4.1 %collective-permute-start.14 = (bf16[2,16,256]{2,1,0:T(8,128)(2,1)S(1)}, bf16[2,16,256]{2,1,0:T(8,128)(2,1)S(1)}, u32[]{:S(2)}, u32[]{:S(2)}) collective-permute-start(bf16[2,16,256]{2,1,0:T(8,128)(2,1)S(1)} %pad_maximum_fusion.1.r0), channel_id=1, source_target_pairs={{0,4},{2,6},{4,0},{6,2},{1,5},{3,7},{5,1},{7,3},{8,12},{10,14},{12... | collective-permute-start | bytes 49160 | tf_op jit(solution)/shard_map/ppermute | solution.py:43
  51.8 3.8 %collective-permute-start.13 = (bf16[2,16,256]{2,1,0:T(8,128)(2,1)S(1)}, bf16[2,16,256]{2,1,0:T(8,128)(2,1)S(1)}, u32[]{:S(2)}, u32[]{:S(2)}) collective-permute-start(bf16[2,16,256]{2,1,0:T(8,128)(2,1)S(1)} %pad_maximum_fusion.1.r0), channel_id=1, source_target_pairs={{0,2},{2,0},{4,6},{6,4},{1,3},{3,1},{5,7},{7,5},{8,10},{10,8},{12,... | collective-permute-start | bytes 49160 | tf_op jit(solution)/shard_map/ppermute | solution.py:43
  82.2 3.9 %collective-permute-start.16 = (bf16[2,16,256]{2,1,0:T(8,128)(2,1)S(1)}, bf16[2,16,256]{2,1,0:T(8,128)(2,1)S(1)}, u32[]{:S(2)}, u32[]{:S(2)}) collective-permute-start(bf16[2,16,256]{2,1,0:T(8,128)(2,1)S(1)} %get-tuple-element.13), channel_id=1, source_target_pairs={{0,2},{2,0},{4,6},{6,4},{1,3},{3,1},{5,7},{7,5},{8,10},{10,8},{12,... | collective-permute-start | bytes 49160 | tf_op jit(solution)/shard_map/ppermute | solution.py:387
  82.3 4.2 %collective-permute-start.17 = (bf16[2,16,256]{2,1,0:T(8,128)(2,1)S(1)}, bf16[2,16,256]{2,1,0:T(8,128)(2,1)S(1)}, u32[]{:S(2)}, u32[]{:S(2)}) collective-permute-start(bf16[2,16,256]{2,1,0:T(8,128)(2,1)S(1)} %get-tuple-element.14), channel_id=1, source_target_pairs={{0,4},{2,6},{4,0},{6,2},{1,5},{3,7},{5,1},{7,3},{8,12},{10,14},{12... | collective-permute-start | bytes 49160 | tf_op jit(solution)/shard_map/ppermute | solution.py:387
  84.6 3.8 %collective-permute-start.18 = (bf16[2,16,256]{2,1,0:T(8,128)(2,1)S(1)}, bf16[2,16,256]{2,1,0:T(8,128)(2,1)S(1)}, u32[]{:S(2)}, u32[]{:S(2)}) collective-permute-start(bf16[2,16,256]{2,1,0:T(8,128)(2,1)S(1)} %get-tuple-element.15), channel_id=1, source_target_pairs={{0,6},{2,4},{4,2},{6,0},{1,7},{3,5},{5,3},{7,1},{8,14},{10,12},{12... | collective-permute-start | bytes 49160 | tf_op jit(solution)/shard_map/ppermute | solution.py:387
  88.4 6.2 %collective-permute-start.19 = (f32[16,256]{1,0:T(8,128)S(1)}, f32[16,256]{1,0:T(8,128)S(1)}, u32[]{:S(2)}, u32[]{:S(2)}) collective-permute-start(f32[16,256]{1,0:T(8,128)S(1)} %get-tuple-element.17), channel_id=1, source_target_pairs={{0,1},{1,0},{2,3},{3,2},{4,5},{5,4},{6,7},{7,6},{8,9},{9,8},{10,11... | collective-permute-start | bytes 49160 | tf_op jit(solution)/shard_map/ppermute | solution.py:408
  (10 other events, 107.0 us)
